TPU v7x, 512 devices: a whole 4x4x16 slice. The times are simulated.
512 devices in a mesh: row: 16 (over y, x), col: 32 (over z, core).
Axes of the slice: x: 4, y: 4, z: 16, core: 2. Of those that a mesh axis runs over, the one named last changes fastest.
Arguments:
- mix_input: bfloat16 [4, 65536, 512], P(None, ('row', 'col')), may hold values from -6 to 6
- group_maps: bfloat16 [4, 128, 128], replicated, may hold values from -0.5 to 0.5
- out_map: bfloat16 [512, 2048], replicated, may hold values from -0.25 to 0.25
Outputs:
- mixed: bfloat16 [4, 65536, 2048], P(None, ('row', 'col'))
All inputs are finite; a program needn't handle non-finite values.
Results may differ from a plain program's by a relative error of at most 0.011.
Values may be sent and summed in bfloat16 or wider, within the bound.
No kernel may reach another device: no remote copies, remote signals or barrier semaphores. Data moves between devices by JAX's collectives and lax.ppermute only.
A program may use at most 64 MiB of HBM per device.

v0:
```python
import math

import jax
import jax.numpy as jnp
from jax import lax
from jax.sharding import PartitionSpec as P

precise = lax.Precision.HIGHEST


def angle_pair(left_ids, right_ids, modulus):
    turn_count = left_ids[:, None] * right_ids[None, :] % modulus
    angles = turn_count.astype(jnp.float32) * (2.0 * math.pi / modulus)
    return (jnp.cos(angles), jnp.sin(angles))


def rotate(real_part, imag_part, cosine, sine_part):
    return (real_part * cosine + imag_part * sine_part, imag_part * cosine - real_part * sine_part)


def transform(real_in, imag_in, cosine, sine_part, einsum_form):
    real_out = jnp.einsum(einsum_form, real_in, cosine, precision=precise) + jnp.einsum(
        einsum_form, imag_in, sine_part, precision=precise
    )
    imag_out = jnp.einsum(einsum_form, imag_in, cosine, precision=precise) - jnp.einsum(
        einsum_form, real_in, sine_part, precision=precise
    )
    return (real_out, imag_out)


def per_device(mix_input, group_maps, out_map):
    sequences, positions, channels = mix_input.shape
    group_count, group_width, _ = group_maps.shape
    row_count = lax.axis_size("row")
    col_count = lax.axis_size("col")
    row_id = lax.axis_index("row")
    col_id = lax.axis_index("col")
    block_span = col_count * positions
    length = row_count * block_span
    norm_factor = 1.0 / math.sqrt(length * group_width)
    width_ids = jnp.arange(group_width, dtype=jnp.int32)
    real_tab, sine_tab = angle_pair(width_ids, width_ids, group_width)
    imag_tab = -sine_tab
    lane_count = real_tab.shape[1]
    signal = mix_input.astype(jnp.float32).reshape(sequences, positions, group_count, group_width)
    real_part = jnp.einsum("spgj,jl->sglp", signal, real_tab, precision=precise)
    imag_part = jnp.einsum("spgj,jl->sglp", signal, imag_tab, precision=precise)
    total_items = sequences * group_count * lane_count
    row_items = total_items // row_count
    dev_items = row_items // col_count
    send_shape = (row_count, row_items, 1, positions)
    col_shape = (col_count, dev_items, row_count, 1, positions)
    row_ids = jnp.arange(row_count, dtype=jnp.int32)
    pos_ids = jnp.arange(positions, dtype=jnp.int32)
    col_ids = jnp.arange(col_count, dtype=jnp.int32)
    row_cos, row_sin = angle_pair(row_ids, row_ids, row_count)
    turn_cos, turn_sin = angle_pair(row_ids, col_id * positions + pos_ids, length)
    col_cos, col_sin = angle_pair(col_ids, col_ids, col_count)
    step_cos, step_sin = angle_pair(col_ids, pos_ids, block_span)
    pos_cos, pos_sin = angle_pair(pos_ids, pos_ids, positions)
    row_send = (real_part.reshape(send_shape), imag_part.reshape(send_shape))
    pieces = (
        lax.all_to_all(
            row_send[0].astype(jnp.bfloat16), "row", split_axis=0, concat_axis=2, tiled=True
        ).astype(jnp.float32),
        lax.all_to_all(
            row_send[1].astype(jnp.bfloat16), "row", split_axis=0, concat_axis=2, tiled=True
        ).astype(jnp.float32),
    )
    spun_pair = transform(pieces[0][0], pieces[1][0], row_cos, row_sin, "nrp,rk->nkp")
    real_out, imag_out = rotate(spun_pair[0], spun_pair[1], turn_cos, turn_sin)
    real_rows = real_out[None]
    imag_rows = imag_out[None]
    pieces = (
        lax.all_to_all(
            real_rows.reshape(col_shape), "col", split_axis=0, concat_axis=3, tiled=True
        ),
        lax.all_to_all(
            imag_rows.reshape(col_shape), "col", split_axis=0, concat_axis=3, tiled=True
        ),
    )
    spun_pair = transform(pieces[0][0], pieces[1][0], col_cos, col_sin, "nacp,cb->nabp")
    turned = rotate(spun_pair[0], spun_pair[1], step_cos, step_sin)
    real_out = jnp.einsum("nabp,pq->nqba", turned[0], pos_cos, precision=precise) + jnp.einsum(
        "nabp,pq->nqba", turned[1], pos_sin, precision=precise
    )
    real_spec = real_out.reshape(1, real_out.shape[0], length)
    spectrum = real_spec[0][:, None]
    spectrum = (spectrum * norm_factor).astype(jnp.bfloat16)
    halves = spectrum.shape[1]
    spectrum = spectrum.reshape(1, dev_items, halves, row_count, col_count, positions)
    returned = lax.all_to_all(spectrum, "col", split_axis=4, concat_axis=0, tiled=True)
    held_groups = sequences * group_count // row_count
    returned = returned.reshape(held_groups, lane_count, halves, row_count, positions)
    full_width = returned[:, :, 0]
    group_ids = (row_id * held_groups + jnp.arange(held_groups, dtype=jnp.int32)) % group_count
    picker = (group_ids[:, None] == jnp.arange(group_count, dtype=jnp.int32)[None, :]).astype(
        jnp.bfloat16
    )
    chosen = jnp.einsum(
        "hg,glm->hlm", picker, group_maps, preferred_element_type=jnp.float32
    ).astype(jnp.bfloat16)
    grouped = jnp.einsum(
        "hlap,hlm->hapm", full_width, chosen, preferred_element_type=jnp.float32
    ).astype(jnp.bfloat16)
    grouped = grouped.reshape(1, held_groups, row_count, positions, group_width)
    arrived = lax.all_to_all(grouped, "row", split_axis=2, concat_axis=0, tiled=True)
    arrived = arrived.reshape(sequences, group_count, positions, group_width)
    mixed_out = jnp.einsum(
        "sgpm,gmn->spn",
        arrived,
        out_map.reshape(group_count, group_width, out_map.shape[1]),
        preferred_element_type=jnp.float32,
    )
    return mixed_out.astype(jnp.bfloat16)


def solution(mesh):
    return jax.shard_map(
        per_device,
        mesh=mesh,
        in_specs=(P(None, ("row", "col"), None), P(), P()),
        out_specs=P(None, ("row", "col"), None),
        check_vma=False,
    )
```

profile of v0, /device:TPU:1, one launch (start us, length us, event | category | flops | bytes accessed | tf_op | source)
XLA Modules:
  0.0 248.9 jit_solution(10785886585991419365)
XLA Ops:
  0.0 2.8 %convolution_convert_fusion.2 = bf16[128,4,128,4]{2,0,3,1:T(8,128)(2,1)} fusion(bf16[4,128,512]{2,1,0:T(8,128)(2,1)} %param.3), kind=kOutput, calls=%fused_computation.10 | convolution fusion | flops 403144704 | bytes 1048576 | tf_op jit(solution)/shard_map/spgj,jl->sglp/dot_general | solution.py:46
  2.8 7.6 %all-to-all-start = ((bf16[16,128,1,128]{3,1,2,0:T(8,128)(2,1)}), bf16[16,128,1,128]{3,1,2,0:T(8,128)(2,1)S(1)}, u32[]{:S(2)}, u32[]{:S(2)}) async-start(bf16[16,128,1,128]{3,1,2,0:T(8,128)(2,1)} %bitcast.155), calls=%async_computation | async-start | bytes 1048576 | tf_op jit(solution)/shard_map/all_to_all | solution.py:63
  10.4 1.6 convolution_convert_fusion.1
  12.1 7.4 %all-to-all-done = bf16[16,128,1,128]{3,1,2,0:T(8,128)(2,1)S(1)} async-done(((bf16[16,128,1,128]{3,1,2,0:T(8,128)(2,1)}), bf16[16,128,1,128]{3,1,2,0:T(8,128)(2,1)S(1)}, u32[]{:S(2)}, u32[]{:S(2)}) %all-to-all-start) | async-done | bytes 524320 | tf_op jit(solution)/shard_map/all_to_all | solution.py:63
  19.5 3.6 %all-to-all-start.1 = ((bf16[16,128,1,128]{3,1,2,0:T(8,128)(2,1)}), bf16[16,128,1,128]{3,1,2,0:T(8,128)(2,1)S(1)}, u32[]{:S(2)}, u32[]{:S(2)}) async-start(bf16[16,128,1,128]{3,1,2,0:T(8,128)(2,1)} %bitcast.154), calls=%async_computation.1 | async-start | bytes 1048576 | tf_op jit(solution)/shard_map/all_to_all | solution.py:66
  23.1 0.1 fusion.104
  23.1 1.7 fusion.26
  24.8 7.4 %all-to-all-done.1 = bf16[16,128,1,128]{3,1,2,0:T(8,128)(2,1)S(1)} async-done(((bf16[16,128,1,128]{3,1,2,0:T(8,128)(2,1)}), bf16[16,128,1,128]{3,1,2,0:T(8,128)(2,1)S(1)}, u32[]{:S(2)}, u32[]{:S(2)}) %all-to-all-start.1) | async-done | bytes 524320 | tf_op jit(solution)/shard_map/all_to_all | solution.py:66
  32.3 0.7 fusion.28
  33.0 0.5 copy-done.2
  33.5 0.8 convolution_add_fusion.2
  34.3 1.9 multiply_add_fusion
  36.2 75.4 %all_to_all.84 = f32[32,4,16,1,128]{4,2,1,3,0:T(8,128)S(1)} all-to-all(f32[32,4,16,1,128]{4,2,1,3,0:T(8,128)S(1)} %bitcast.152), channel_id=1, replica_groups=mesh['row'=16,'col'=32] {'col'}, dimensions={0} | all-to-all | bytes 2097152 | tf_op jit(solution)/shard_map/all_to_all | solution.py:75
  111.5 4.8 %all-to-all-start.3 = ((f32[32,4,16,1,128]{4,2,1,3,0:T(8,128)}), f32[32,4,16,1,128]{4,2,1,3,0:T(8,128)}, u32[]{:S(2)}, u32[]{:S(2)}) async-start(f32[32,4,16,1,128]{4,2,1,3,0:T(8,128)} %bitcast.151), calls=%async_computation.3 | async-start | bytes 2097152 | tf_op jit(solution)/shard_map/all_to_all | solution.py:78
  116.3 0.1 fusion.89
  116.4 2.6 %fusion.8 = f32[32,4,16,128]{3,0,2,1:T(8,128)} fusion(f32[32,4,16,1,128]{4,2,1,3,0:T(8,128)S(1)} %all_to_all.84), kind=kOutput, calls=%fused_computation.17 | convolution fusion | flops 100677632 | bytes 2097152 | tf_op jit(solution)/shard_map/nacp,cb->nabp/dot_general | solution.py:22
  119.0 53.1 %all-to-all-done.3 = f32[32,4,16,1,128]{4,2,1,3,0:T(8,128)} async-done(((f32[32,4,16,1,128]{4,2,1,3,0:T(8,128)}), f32[32,4,16,1,128]{4,2,1,3,0:T(8,128)}, u32[]{:S(2)}, u32[]{:S(2)}) %all-to-all-start.3) | async-done | bytes 1048608 | tf_op jit(solution)/shard_map/all_to_all | solution.py:78
  172.2 2.9 %fusion.10 = f32[32,4,16,128]{3,0,2,1:T(8,128)S(1)} fusion(f32[32,4,16,1,128]{4,2,1,3,0:T(8,128)} %all-to-all-done.3), kind=kOutput, calls=%fused_computation.19 | convolution fusion | flops 100677632 | bytes 2097152 | tf_op jit(solution)/shard_map/nacp,cb->nabp/dot_general | solution.py:25
  175.1 2.8 %convolution_add_fusion.1 = f32[32,4,16,128]{3,0,2,1:T(8,128)S(1)} fusion(f32[32,4,16,128]{3,0,2,1:T(8,128)S(1)} %copy-done.1, f32[32,4,16,1,128]{4,2,1,3,0:T(8,128)} %all-to-all-done.3), kind=kOutput, calls=%fused_computation.4 | convolution fusion | flops 100939776 | bytes 3145728 | tf_op jit(solution)/shard_map/nacp,cb->nabp/dot_general | solution.py:22
  177.9 1.6 convolution_subtract_fusion
  179.5 1.2 fusion.5
  180.7 1.2 fusion.3
  182.0 6.5 %copy.35 = bf16[4,128,32,16]{3,2,1,0:T(8,128)(2,1)} copy(bf16[4,128,32,16]{1,2,3,0:T(8,128)(2,1)S(1)} %fusion.3) | data formatting | bytes 1048576 | tf_op jit(solution)/shard_map/convert_element_type | solution.py:89
  188.5 5.1 %convert_element_type.134 = bf16[1,4,1,16,32,128]{5,4,3,1,2,0:T(8,128)(2,1)S(1)} reshape(bf16[4,128,32,16]{3,2,1,0:T(8,128)(2,1)} %copy.35) | data formatting | bytes 1048576 | tf_op jit(solution)/shard_map/convert_element_type | solution.py:89
  193.6 0.0 copy-start.4
  193.6 1.0 copy.36
  194.6 4.6 %all-to-all-start.4 = ((bf16[1,4,1,16,32,128]{5,3,1,2,0,4:T(8,128)(2,1)}), bf16[1,4,1,16,32,128]{5,3,1,2,0,4:T(8,128)(2,1)S(1)}, u32[]{:S(2)}, u32[]{:S(2)}) async-start(bf16[1,4,1,16,32,128]{5,3,1,2,0,4:T(8,128)(2,1)} %copy.36), calls=%async_computation.4 | async-start | bytes 1048576 | tf_op jit(solution)/shard_map/all_to_all | solution.py:92
  199.2 0.2 fusion.42
  199.4 33.3 %all-to-all-done.4 = bf16[1,4,1,16,32,128]{5,3,1,2,0,4:T(8,128)(2,1)S(1)} async-done(((bf16[1,4,1,16,32,128]{5,3,1,2,0,4:T(8,128)(2,1)}), bf16[1,4,1,16,32,128]{5,3,1,2,0,4:T(8,128)(2,1)S(1)}, u32[]{:S(2)}, u32[]{:S(2)}) %all-to-all-start.4) | async-done | bytes 524320 | tf_op jit(solution)/shard_map/all_to_all | solution.py:92
  232.7 0.3 fusion.2
  233.0 13.2 %all_to_all.85 = bf16[1,1,16,128,128]{4,3,1,0,2:T(8,128)(2,1)S(1)} all-to-all(bf16[1,1,16,128,128]{4,3,1,0,2:T(8,128)(2,1)S(1)} %fusion.2), channel_id=1, replica_groups=mesh['row'=16,'col'=32] {'row'}, dimensions={2} | all-to-all | bytes 1048576 | tf_op jit(solution)/shard_map/all_to_all | solution.py:107
  246.3 2.6 %bitcast_convert_fusion = bf16[4,128,2048]{2,1,0:T(8,128)(2,1)} fusion(bf16[4,4,128,128]{3,2,1,0:T(8,128)(2,1)S(1)} %bitcast.156, bf16[4,128,2048,1]{2,1,0,3:T(8,128)(2,1)S(1)} %bitcast.150), kind=kOutput, calls=%fused_computation | convolution fusion | flops 1074790400 | bytes 4718592 | tf_op jit(solution)/shard_map/sgpm,gmn->spn/dot_general | solution.py:109
  (9 shorter events, 0.0 us)
Async XLA Ops:
  0.0 246.3 %copy-start = (bf16[512,2048]{1,0:T(8,128)(2,1)S(1)}, bf16[512,2048]{1,0:T(8,128)(2,1)}, u32[]{:S(2)}) copy-start(bf16[512,2048]{1,0:T(8,128)(2,1)} %param.5) | copy-start | bytes 6291460
  0.0 10.4 %copy-start.3 = (bf16[4,128,512]{2,1,0:T(8,128)(2,1)S(1)}, bf16[4,128,512]{2,1,0:T(8,128)(2,1)}, u32[]{:S(2)}) copy-start(bf16[4,128,512]{2,1,0:T(8,128)(2,1)} %param.3) | copy-start | bytes 1572868
  2.8 16.6 %all-to-all-start = ((bf16[16,128,1,128]{3,1,2,0:T(8,128)(2,1)}), bf16[16,128,1,128]{3,1,2,0:T(8,128)(2,1)S(1)}, u32[]{:S(2)}, u32[]{:S(2)}) async-start(bf16[16,128,1,128]{3,1,2,0:T(8,128)(2,1)} %bitcast.155), calls=%async_computation | async-start | bytes 1048576 | tf_op jit(solution)/shard_map/all_to_all | solution.py:63
  19.5 12.8 %all-to-all-start.1 = ((bf16[16,128,1,128]{3,1,2,0:T(8,128)(2,1)}), bf16[16,128,1,128]{3,1,2,0:T(8,128)(2,1)S(1)}, u32[]{:S(2)}, u32[]{:S(2)}) async-start(bf16[16,128,1,128]{3,1,2,0:T(8,128)(2,1)} %bitcast.154), calls=%async_computation.1 | async-start | bytes 1048576 | tf_op jit(solution)/shard_map/all_to_all | solution.py:66
  32.3 1.2 copy-start.2
  111.5 60.6 %all-to-all-start.3 = ((f32[32,4,16,1,128]{4,2,1,3,0:T(8,128)}), f32[32,4,16,1,128]{4,2,1,3,0:T(8,128)}, u32[]{:S(2)}, u32[]{:S(2)}) async-start(f32[32,4,16,1,128]{4,2,1,3,0:T(8,128)} %bitcast.151), calls=%async_computation.3 | async-start | bytes 2097152 | tf_op jit(solution)/shard_map/all_to_all | solution.py:78
  172.2 2.9 %copy-start.1 = (f32[32,4,16,128]{3,0,2,1:T(8,128)S(1)}, f32[32,4,16,128]{3,0,2,1:T(8,128)}, u32[]{:S(2)}) copy-start(f32[32,4,16,128]{3,0,2,1:T(8,128)} %fusion.8) | copy-start | bytes 3145732
  193.6 5.6 %copy-start.4 = (bf16[4,128,128]{2,1,0:T(8,128)(2,1)S(1)}, bf16[4,128,128]{2,1,0:T(8,128)(2,1)}, u32[]{:S(2)}) copy-start(bf16[4,128,128]{2,1,0:T(8,128)(2,1)} %param.4) | copy-start | bytes 393220
  194.6 38.1 %all-to-all-start.4 = ((bf16[1,4,1,16,32,128]{5,3,1,2,0,4:T(8,128)(2,1)}), bf16[1,4,1,16,32,128]{5,3,1,2,0,4:T(8,128)(2,1)S(1)}, u32[]{:S(2)}, u32[]{:S(2)}) async-start(bf16[1,4,1,16,32,128]{5,3,1,2,0,4:T(8,128)(2,1)} %copy.36), calls=%async_computation.4 | async-start | bytes 1048576 | tf_op jit(solution)/shard_map/all_to_all | solution.py:92
where the time goes:
time: 250 us; the launch traced here: 249 us
  waiting for transfers between devices  101 us (40%)
  blocking collectives  88.6 us (35%)
  matrix products  25.1 us (10%)
  starting transfers between devices  20.5 us (8%)
  local copies, waits for them, and re-layouts  13.1 us (5%)
    all_to_all x1, blocking collectives, per_device(): lax.all_to_all(real_rows.reshape(col_shape), 'col', split_axis=0, concat_...  75.4 us
    all_to_all x1, waiting for transfers between devices, per_device(): lax.all_to_all(imag_rows.reshape(col_shape), 'col', split_axis=0, concat_...  53.1 us
    all_to_all x1, waiting for transfers between devices, per_device(): lax.all_to_all(spectrum, 'col', split_axis=4, concat_axis=0, tiled=True)  33.3 us
    all_to_all x1, blocking collectives, per_device(): lax.all_to_all(grouped, 'row', split_axis=2, concat_axis=0, tiled=True)  13.2 us
    convert_element_type x3, local copies, waits for them, and re-layouts, per_device(): spectrum = (spectrum * norm_factor).astype(jnp.bfloat16)  12.6 us
    all_to_all x1, starting transfers between devices, per_device(): lax.all_to_all(row_send[0].astype(jnp.bfloat16), 'row', split_axis=0, con...  7.57 us
    all_to_all x1, waiting for transfers between devices, per_device(): lax.all_to_all(row_send[1].astype(jnp.bfloat16), 'row', split_axis=0, con...  7.44 us
    all_to_all x1, waiting for transfers between devices, per_device(): lax.all_to_all(row_send[0].astype(jnp.bfloat16), 'row', split_axis=0, con...  7.38 us
  transfers between devices with their start and end apart: 4, of which 4 were waited for; matrix products, arithmetic and copies ran while one was open for 3% of the time, Pallas kernels for 0%

commit v1 on v0

v1 whole, which is shorter than its diff:
```python
import functools
import math

import jax
import jax.numpy as jnp
import numpy as np
from jax import lax
from jax.experimental import pallas as pl
from jax.experimental.pallas import tpu as pltpu
from jax.sharding import PartitionSpec as P

AXES = ("row", "col")
F32, BF16 = jnp.float32, jnp.bfloat16
NT = (((1,), (1,)), ((), ()))


def turns(left, right, modulus):
    angle = np.outer(left, right) % modulus * (2.0 * math.pi / modulus)
    return np.cos(angle), np.sin(angle)


def channel_table(width):
    cosine, sine = turns(np.arange(width // 2), np.arange(width), width)
    sine[0] = np.cos(np.pi * np.arange(width))
    return np.stack([cosine, sine], axis=1).reshape(width, width)


def frequency_of_item(width):
    slots = np.arange(width // 2)
    mirrored = np.where(slots == 0, width // 2, width - slots)
    return np.stack([slots, mirrored], axis=1).reshape(width)


def coarse_table(count):
    half = np.arange(count // 2)
    ids = np.concatenate([np.arange(0, count, 2), np.arange(1, count, 2)])
    return np.concatenate(turns(half, ids, count), axis=0)


def fine_table(count):
    cosine, sine = turns(np.arange(count), np.arange(count), count)
    zero = np.zeros_like(cosine)
    plain = np.block([[cosine, -sine, -sine, -cosine], [cosine, sine, -sine, cosine]])
    edge = np.block([[cosine, zero, -sine, zero], [zero, cosine, zero, -sine]])
    return np.stack([plain, edge])


def channel_kernel(table_ref, signal_ref, out_ref):
    sequences, _, channels = signal_ref.shape
    width = table_ref.shape[0]
    for item in range(sequences * channels // width):
        seq, group = divmod(item, channels // width)
        block = signal_ref[seq, :, group * width : (group + 1) * width]
        mapped = lax.dot_general(table_ref[...], block, NT, preferred_element_type=F32)
        out_ref[item * width : (item + 1) * width, :] = mapped.astype(BF16)


def position_kernel(flag_ref, items_ref, coarse_ref, twist_ref, fine_ref, out_ref, wide_ref, spun_ref):
    rows, lanes = items_ref.shape
    blocks = rows // 4
    half = blocks // 2
    wide_ref[...] = items_ref[...].astype(F32)
    results = []
    for slot in range(2):

        def gather(parity):
            pieces = [
                wide_ref[pl.ds(4 * parity + 2 * slot + part, half, stride=8), :].astype(BF16)
                for part in range(2)
            ]
            return jnp.concatenate(pieces, axis=1)

        even = jnp.dot(coarse_ref[:, :half], gather(0), preferred_element_type=F32)
        odd = jnp.dot(coarse_ref[:, half:], gather(1), preferred_element_type=F32)
        for top in range(2):
            total = even - odd if top else even + odd
            cos_sum, sin_sum = total[:half], total[half:]
            turn_cos = twist_ref[0, top * half : (top + 1) * half, :]
            turn_sin = twist_ref[1, top * half : (top + 1) * half, :]
            turn_cos = jnp.concatenate([turn_cos, turn_cos], axis=1)
            turn_sin = jnp.concatenate([turn_sin, turn_sin], axis=1)
            spun_ref[slot, top * half : (top + 1) * half, : 2 * lanes] = (
                cos_sum * turn_cos - sin_sum * turn_sin
            ).astype(BF16)
            spun_ref[slot, top * half : (top + 1) * half, 2 * lanes :] = (
                cos_sum * turn_sin + sin_sum * turn_cos
            ).astype(BF16)
    for slot in range(2):
        table = fine_ref[flag_ref[0]] if slot == 0 else fine_ref[0]
        result = lax.dot_general(table, spun_ref[slot], NT, preferred_element_type=F32)
        for part in range(2):
            for quarter in range(blocks // lanes):
                wide_ref[pl.ds(4 * quarter + 2 * slot + part, lanes, stride=4 * (blocks // lanes)), :] = result[
                    part * lanes : (part + 1) * lanes, quarter * lanes : (quarter + 1) * lanes
                ]
    out_ref[...] = wide_ref[...].astype(BF16)


def map_kernel(spec_ref, maps_ref, out_map_ref, out_ref):
    groups, width, _ = maps_ref.shape
    for seq in range(out_ref.shape[0]):
        pieces = []
        for group in range(groups):
            start = (seq * groups + group) * width
            block = spec_ref[start : start + width, :]
            mapped = lax.dot_general(
                block, maps_ref[group], (((0,), (0,)), ((), ())), preferred_element_type=F32
            )
            pieces.append(mapped.astype(BF16))
        grouped = jnp.concatenate(pieces, axis=1)
        out_ref[seq] = jnp.dot(grouped, out_map_ref[...], preferred_element_type=F32).astype(BF16)


def call(kernel, shape, dtype, scratch=(), smem=0, count=1, limit=None):
    specs = [pl.BlockSpec(memory_space=pltpu.SMEM)] * smem
    specs += [pl.BlockSpec(memory_space=pltpu.VMEM)] * (count - smem)
    return pl.pallas_call(
        kernel,
        out_shape=jax.ShapeDtypeStruct(shape, dtype),
        in_specs=specs,
        out_specs=pl.BlockSpec(memory_space=pltpu.VMEM),
        scratch_shapes=list(scratch),
        compiler_params=pltpu.CompilerParams(vmem_limit_bytes=limit),
    )


def exchange(rows, devices):
    sent = rows.reshape(devices, rows.shape[0] // devices, rows.shape[1])
    return lax.all_to_all(sent, AXES, split_axis=0, concat_axis=0, tiled=True).reshape(rows.shape)


def per_device(mix_input, group_maps, out_map):
    sequences, positions, channels = mix_input.shape
    groups, width, _ = group_maps.shape
    devices = lax.axis_size("row") * lax.axis_size("col")
    length = devices * positions
    rows = sequences * channels
    assert rows == 4 * devices and positions == width and devices == 4 * positions

    def table(values):
        return np.asarray(values, dtype=np.float32).astype(BF16)

    norm = 1.0 / math.sqrt(length * width)
    twist = norm * np.stack(turns(np.arange(devices), np.arange(positions), length))
    picker = np.eye(width)[frequency_of_item(width)]
    first = (lax.axis_index("col") == 0).astype(jnp.int32).reshape(1)

    items = call(channel_kernel, (rows, positions), BF16, count=2, limit=8 << 20)(
        table(channel_table(width)), mix_input
    )
    items = exchange(items, devices)
    spectrum = call(
        position_kernel,
        (rows, positions),
        BF16,
        scratch=(pltpu.VMEM((rows, positions), F32), pltpu.VMEM((2, devices, 4 * positions), BF16)),
        smem=1,
        count=5,
        limit=24 << 20,
    )(first, items, table(coarse_table(devices)), twist.astype(np.float32), table(fine_table(positions)))
    spectrum = exchange(spectrum, devices)
    maps = jnp.einsum("tl,glm->gtm", table(picker), group_maps, preferred_element_type=F32).astype(BF16)
    return call(
        map_kernel, (sequences, positions, out_map.shape[1]), BF16, count=3, limit=24 << 20
    )(spectrum, maps, out_map)


def solution(mesh):
    return jax.shard_map(
        per_device,
        mesh=mesh,
        in_specs=(P(None, AXES, None), P(), P()),
        out_specs=P(None, AXES, None),
        check_vma=False,
    )
```

time: 250 us -> 115 us (0.46)
  blocking collectives: 88.6 us -> 0 us
  waiting for transfers between devices: 101 us -> 70.9 us
  matrix products: 25.1 us -> 0.17 us
  starting transfers between devices: 20.5 us -> 32.7 us
  local copies, waits for them, and re-layouts: 13.1 us -> 3.94 us
  Pallas kernels: 0 us -> 6.49 us
    all_to_all x2 -> x0, blocking collectives: 88.6 us -> none  [the longest x1 75.4 us: per_device(): lax.all_to_all(real_rows.reshape(col_shape), 'col', split_axis=0, concat_...]
    all_to_all x4 -> x2, waiting for transfers between devices: 101 us -> 70.9 us  [exchange(): lax.all_to_all(sent, AXES, split_axis=0, concat_axis=0, tiled=True)]
    dot_general x15 -> x1, matrix products: 25.1 us -> 0.17 us  [per_device(): jnp.einsum('tl,glm->gtm', table(picker), group_maps, preferred_element_ty...]
    convert_element_type x3 -> x0, local copies, waits for them, and re-layouts: 12.6 us -> none  [per_device(): spectrum = (spectrum * norm_factor).astype(jnp.bfloat16)]
    all_to_all x4 -> x2, starting transfers between devices: 20.5 us -> 32.7 us  [exchange(): lax.all_to_all(sent, AXES, split_axis=0, concat_axis=0, tiled=True)]
    pallas_call x0 -> x3, Pallas kernels: none -> 6.49 us  [the longest x1 3.17 us: per_device(): call(map_kernel, (sequences, positions, out_map.shape[1]), BF16, count=3,...]
    unnamed x10 -> x16, local copies, waits for them, and re-layouts: 0.51 us -> 3.94 us
  transfers between devices with their start and end apart: 4 -> 2, of which waited for: 4 -> 2; matrix products, arithmetic and copies ran while one was open for 3% -> 0% of each run, Pallas kernels for 0% -> 0%
where the time goes in v1:
time: 115 us; the launch traced here: 114 us
  waiting for transfers between devices  70.9 us (62%)
  starting transfers between devices  32.7 us (28%)
  Pallas kernels  6.49 us (6%)
  local copies, waits for them, and re-layouts  3.94 us (3%)
    all_to_all x2, waiting for transfers between devices, exchange(): lax.all_to_all(sent, AXES, split_axis=0, concat_axis=0, tiled=True)  70.9 us
    all_to_all x2, starting transfers between devices, exchange(): lax.all_to_all(sent, AXES, split_axis=0, concat_axis=0, tiled=True)  32.7 us
    unnamed x16, local copies, waits for them, and re-layouts  3.94 us
    pallas_call x1, Pallas kernels, per_device(): call(map_kernel, (sequences, positions, out_map.shape[1]), BF16, count=3,...  3.17 us
  transfers between devices with their start and end apart: 2, of which 2 were waited for; matrix products, arithmetic and copies ran while one was open for 0% of the time, Pallas kernels for 0%

profile of v1, /device:TPU:1, one launch (start us, length us, event | category | flops | bytes accessed | tf_op | source)
XLA Modules:
  0.0 114.2 jit_solution(17335636320811253946)
XLA Ops:
  0.0 0.0 copy-start
  0.0 0.0 copy-start.2
  0.0 1.1 copy-done.2
  1.1 0.0 copy-start.6
  1.1 0.8 copy-done.6
  1.8 0.0 copy-start.3
  1.8 1.3 %shard_map.82 = bf16[2048,128]{1,0:T(8,128)(2,1)} custom-call(bf16[128,128]{1,0:T(8,128)(2,1)S(1)} %copy-done.6, bf16[4,128,512]{2,1,0:T(8,128)(2,1)S(1)} %copy-done.2), custom_call_target="tpu_custom_call" | custom-call | tf_op jit(solution)/shard_map/pallas_call | solution.py:148
  3.1 0.0 copy-start.7
  3.1 24.3 %all-to-all-start = ((bf16[512,4,128]{2,1,0:T(4,128)(2,1)}), bf16[512,4,128]{2,1,0:T(4,128)(2,1)S(1)}, u32[]{:S(2)}, u32[]{:S(2)}) async-start(bf16[512,4,128]{2,1,0:T(4,128)(2,1)} %bitcast.1), calls=%async_computation | async-start | bytes 1048576 | tf_op jit(solution)/shard_map/all_to_all | solution.py:129
  27.4 0.0 copy-start.1
  27.4 35.6 %all-to-all-done = bf16[512,4,128]{2,1,0:T(4,128)(2,1)S(1)} async-done(((bf16[512,4,128]{2,1,0:T(4,128)(2,1)}), bf16[512,4,128]{2,1,0:T(4,128)(2,1)S(1)}, u32[]{:S(2)}, u32[]{:S(2)}) %all-to-all-start) | async-done | bytes 524320 | tf_op jit(solution)/shard_map/all_to_all | solution.py:129
  63.1 0.0 copy-done.3
  63.1 0.0 copy-start.4
  63.1 1.0 copy-done.4
  64.1 0.0 copy-start.5
  64.1 1.0 copy-done.5
  65.2 2.1 %shard_map.83 = bf16[2048,128]{1,0:T(8,128)(2,1)} custom-call(s32[1]{0:T(128)} %bitcast.flag_ref, bf16[2048,128]{1,0:T(8,128)(2,1)S(1)} %bitcast.11, bf16[512,512]{1,0:T(8,128)(2,1)S(1)} %copy-done.5, f32[2,512,128]{2,1,0:T(8,128)S(1)} %copy-done.4, bf16[2,256,512]{2,1,0:T(8,128)(2,1)S(1)} %copy-done.3), custom_call_target="tpu_custom_call" | custom-call | tf_op jit(solution)/shard_map/pallas_call | solution.py:152
  67.2 8.4 %all-to-all-start.1 = ((bf16[512,4,128]{2,1,0:T(4,128)(2,1)}), bf16[512,4,128]{2,1,0:T(4,128)(2,1)S(1)}, u32[]{:S(2)}, u32[]{:S(2)}) async-start(bf16[512,4,128]{2,1,0:T(4,128)(2,1)} %bitcast.3), calls=%async_computation.1 | async-start | bytes 1048576 | tf_op jit(solution)/shard_map/all_to_all | solution.py:129
  75.6 0.0 copy-done
  75.6 0.0 copy-done.7
  75.6 0.2 fusion.maps_ref
  75.8 35.3 %all-to-all-done.1 = bf16[512,4,128]{2,1,0:T(4,128)(2,1)S(1)} async-done(((bf16[512,4,128]{2,1,0:T(4,128)(2,1)}), bf16[512,4,128]{2,1,0:T(4,128)(2,1)S(1)}, u32[]{:S(2)}, u32[]{:S(2)}) %all-to-all-start.1) | async-done | bytes 524320 | tf_op jit(solution)/shard_map/all_to_all | solution.py:129
  111.1 0.0 copy-done.1
  111.1 3.2 %shard_map.84 = bf16[4,128,2048]{2,1,0:T(8,128)(2,1)} custom-call(bf16[2048,128]{1,0:T(8,128)(2,1)S(1)} %bitcast.10, bf16[4,128,128]{2,1,0:T(8,128)(2,1)S(1)} %fusion.maps_ref, bf16[512,2048]{1,0:T(8,128)(2,1)S(1)} %copy-done.1), custom_call_target="tpu_custom_call" | custom-call | tf_op jit(solution)/shard_map/pallas_call | solution.py:163
Async XLA Ops:
  0.0 75.6 %copy-start = (bf16[4,128,128]{2,1,0:T(8,128)(2,1)S(1)}, bf16[4,128,128]{2,1,0:T(8,128)(2,1)}, u32[]{:S(2)}) copy-start(bf16[4,128,128]{2,1,0:T(8,128)(2,1)} %param.9) | copy-start | bytes 393220
  0.0 1.1 copy-start.2
  1.1 0.8 copy-start.6
  1.8 61.2 %copy-start.3 = (bf16[2,256,512]{2,1,0:T(8,128)(2,1)S(1)}, bf16[2,256,512]{2,1,0:T(8,128)(2,1)}, u32[]{:S(2)}) copy-start(bf16[2,256,512]{2,1,0:T(8,128)(2,1)} %constant.19.clone.fine_ref) | copy-start | bytes 1572868
  3.1 72.5 %copy-start.7 = (bf16[128,128,1]{1,0,2:T(8,128)(2,1)S(1)}, bf16[128,128,1]{1,0,2:T(8,128)(2,1)}, u32[]{:S(2)}) copy-start(bf16[128,128,1]{1,0,2:T(8,128)(2,1)} %constant.22) | copy-start | bytes 98308
  3.1 60.0 %all-to-all-start = ((bf16[512,4,128]{2,1,0:T(4,128)(2,1)}), bf16[512,4,128]{2,1,0:T(4,128)(2,1)S(1)}, u32[]{:S(2)}, u32[]{:S(2)}) async-start(bf16[512,4,128]{2,1,0:T(4,128)(2,1)} %bitcast.1), calls=%async_computation | async-start | bytes 1048576 | tf_op jit(solution)/shard_map/all_to_all | solution.py:129
  27.4 83.6 %copy-start.1 = (bf16[512,2048]{1,0:T(8,128)(2,1)S(1)}, bf16[512,2048]{1,0:T(8,128)(2,1)}, u32[]{:S(2)}) copy-start(bf16[512,2048]{1,0:T(8,128)(2,1)} %out_map_ref.1) | copy-start | bytes 6291460
  63.1 1.0 copy-start.4
  64.1 1.0 copy-start.5
  67.2 43.9 %all-to-all-start.1 = ((bf16[512,4,128]{2,1,0:T(4,128)(2,1)}), bf16[512,4,128]{2,1,0:T(4,128)(2,1)S(1)}, u32[]{:S(2)}, u32[]{:S(2)}) async-start(bf16[512,4,128]{2,1,0:T(4,128)(2,1)} %bitcast.3), calls=%async_computation.1 | async-start | bytes 1048576 | tf_op jit(solution)/shard_map/all_to_all | solution.py:129

commit v2 on v1

v2 whole, which is shorter than its diff:
```python
import functools
import math

import jax
import jax.numpy as jnp
import numpy as np
from jax import lax
from jax.experimental import pallas as pl
from jax.experimental.pallas import tpu as pltpu
from jax.sharding import PartitionSpec as P

AXES = ("row", "col")
FAST = pltpu.VMEM
F32, BF16 = jnp.float32, jnp.bfloat16
NT = (((1,), (1,)), ((), ()))


def turns(left, right, modulus):
    angle = np.outer(left, right) % modulus * (2.0 * math.pi / modulus)
    return np.cos(angle), np.sin(angle)


def channel_table(width):
    cosine, sine = turns(np.arange(width // 2), np.arange(width), width)
    sine[0] = np.cos(np.pi * np.arange(width))
    return np.stack([cosine, sine], axis=1).reshape(width, width)


def frequency_of_item(width):
    slots = np.arange(width // 2)
    mirrored = np.where(slots == 0, width // 2, width - slots)
    return np.stack([slots, mirrored], axis=1).reshape(width)


def coarse_table(count):
    half = np.arange(count // 2)
    ids = np.concatenate([np.arange(0, count, 2), np.arange(1, count, 2)])
    return np.concatenate(turns(half, ids, count), axis=0)


def fine_tables(count):
    cosine, sine = turns(np.arange(count), np.arange(count), count)
    return np.stack([np.block([[cosine, -sine]]), np.block([[-sine, -cosine]])])


def channel_kernel(table_hbm, signal_hbm, out_ref, table_ref, signal_ref, sems):
    sequences, _, channels = signal_ref.shape
    width = table_ref.shape[0]
    groups = channels // width
    table_copy = pltpu.make_async_copy(table_hbm, table_ref, sems.at[sequences])
    table_copy.start()
    copies = []
    for seq in range(sequences):
        copies.append(pltpu.make_async_copy(signal_hbm.at[seq], signal_ref.at[seq], sems.at[seq]))
        copies[seq].start()
    table_copy.wait()
    for seq in range(sequences):
        copies[seq].wait()
        for group in range(groups):
            block = signal_ref[seq, :, group * width : (group + 1) * width]
            mapped = lax.dot_general(table_ref[...], block, NT, preferred_element_type=F32)
            start = (seq * groups + group) * width
            out_ref[start : start + width, :] = mapped.astype(BF16)


def fetch(sources, targets, sems):
    copies = [pltpu.make_async_copy(src, dst, sems.at[at]) for at, (src, dst) in enumerate(zip(sources, targets))]
    for copy in copies:
        copy.start()
    for copy in copies:
        copy.wait()


def table_kernel(after_hbm, coarse_hbm, twist_hbm, fine_hbm, coarse_ref, twist_ref, fine_ref, sems):
    fetch((coarse_hbm, twist_hbm, fine_hbm), (coarse_ref, twist_ref, fine_ref), sems)


def weight_kernel(after_hbm, picker_hbm, maps_hbm, out_map_hbm, moved_ref, out_map_ref, picker_ref, maps_ref, sems):
    fetch((picker_hbm, maps_hbm, out_map_hbm), (picker_ref, maps_ref, out_map_ref), sems)
    for group in range(maps_ref.shape[0]):
        moved_ref[group] = jnp.dot(picker_ref[...], maps_ref[group], preferred_element_type=F32).astype(BF16)


def position_kernel(edge_ref, items_ref, coarse_ref, twist_ref, fine_ref, out_ref, wide_ref, spun_ref):
    rows, lanes = items_ref.shape
    blocks = rows // 4
    half = blocks // 2
    quarters = blocks // lanes
    edge = edge_ref[0]
    wide_ref[...] = items_ref[...].astype(F32)
    for slot in range(2):

        def gather(parity):
            pieces = [
                wide_ref[pl.ds(4 * parity + 2 * slot + part, half, stride=8), :].astype(BF16)
                for part in range(2)
            ]
            return jnp.concatenate(pieces, axis=1)

        even = jnp.dot(coarse_ref[:, :half], gather(0), preferred_element_type=F32)
        odd = jnp.dot(coarse_ref[:, half:], gather(1), preferred_element_type=F32)
        for top in range(2):
            total = even - odd if top else even + odd
            span = slice(top * half, (top + 1) * half)
            turn_cos, turn_sin = twist_ref[0, span, :], twist_ref[1, span, :]
            for part in range(2):
                columns = slice(part * lanes, (part + 1) * lanes)
                cos_sum, sin_sum = total[:half, columns], total[half:, columns]
                spun_ref[2 * slot + part, span, :lanes] = (cos_sum * turn_cos - sin_sum * turn_sin).astype(BF16)
                spun_ref[2 * slot + part, span, lanes:] = (cos_sum * turn_sin + sin_sum * turn_cos).astype(BF16)
    for slot in range(2):
        odd_table = fine_ref[1 - edge] if slot == 0 else fine_ref[1]
        even = lax.dot_general(fine_ref[0], spun_ref[2 * slot], NT, preferred_element_type=F32)
        odd = lax.dot_general(odd_table, spun_ref[2 * slot + 1], NT, preferred_element_type=F32)
        if slot == 0:
            results = (jnp.where(edge == 1, even, even + odd), jnp.where(edge == 1, odd, even - odd))
        else:
            results = (even + odd, even - odd)
        for part in range(2):
            for quarter in range(quarters):
                wide_ref[pl.ds(4 * quarter + 2 * slot + part, lanes, stride=4 * quarters), :] = results[part][
                    :, quarter * lanes : (quarter + 1) * lanes
                ]
    out_ref[...] = wide_ref[...].astype(BF16)


def map_kernel(spec_ref, maps_ref, out_map_ref, out_hbm, grouped_ref, mixed_ref, sems):
    groups, width, _ = maps_ref.shape
    sequences, positions, _ = out_hbm.shape
    for seq in range(sequences):
        for group in range(groups):
            start = (seq * groups + group) * width
            block = spec_ref[start : start + width, :]
            mapped = lax.dot_general(
                block, maps_ref[group], (((0,), (0,)), ((), ())), preferred_element_type=F32
            )
            grouped_ref[seq * positions : (seq + 1) * positions, group * width : (group + 1) * width] = (
                mapped.astype(BF16)
            )
    pieces, _, _, span = mixed_ref.shape
    copies = []
    for piece in range(pieces):
        columns = slice(piece * span, (piece + 1) * span)
        mixed = jnp.dot(grouped_ref[...], out_map_ref[:, columns], preferred_element_type=F32)
        mixed_ref[piece] = mixed.astype(BF16).reshape(sequences, positions, span)
        copies.append(pltpu.make_async_copy(mixed_ref.at[piece], out_hbm.at[:, :, columns], sems.at[piece]))
        copies[piece].start()
    for copy in copies:
        copy.wait()


HBM = pl.BlockSpec(memory_space=pl.ANY)
NEAR = pl.BlockSpec(memory_space=pltpu.VMEM)
SCALAR = pl.BlockSpec(memory_space=pltpu.SMEM)


def call(kernel, out_shape, in_specs, out_specs, scratch=(), limit=None, flops=0):
    return pl.pallas_call(
        kernel,
        out_shape=out_shape,
        in_specs=in_specs,
        out_specs=out_specs,
        scratch_shapes=list(scratch),
        cost_estimate=pl.CostEstimate(flops=flops, bytes_accessed=1 << 20, transcendentals=0),
        compiler_params=pltpu.CompilerParams(vmem_limit_bytes=limit),
    )


def exchange(rows, devices):
    sent = rows.reshape(devices, rows.shape[0] // devices, rows.shape[1])
    return lax.all_to_all(sent, AXES, split_axis=0, concat_axis=0, tiled=True).reshape(rows.shape)


def per_device(mix_input, group_maps, out_map):
    sequences, positions, channels = mix_input.shape
    groups, width, _ = group_maps.shape
    devices = lax.axis_size("row") * lax.axis_size("col")
    length = devices * positions
    rows = sequences * channels
    assert rows == 4 * devices and positions == width and devices == 4 * positions

    def table(values):
        return np.asarray(values, dtype=np.float32).astype(BF16)

    norm = 1.0 / math.sqrt(length * width)
    twist = norm * np.stack(turns(np.arange(devices), np.arange(positions), length))
    picker = np.eye(width)[frequency_of_item(width)]
    first = (lax.axis_index("col") == 0).astype(jnp.int32).reshape(1)

    maps_shape = group_maps.shape
    items = call(
        channel_kernel,
        FAST((rows, positions), BF16),
        [HBM, HBM],
        NEAR,
        scratch=(
            pltpu.VMEM((width, width), BF16),
            pltpu.VMEM(mix_input.shape, BF16),
            pltpu.SemaphoreType.DMA((sequences + 1,)),
        ),
        limit=60 << 20,
    )(table(channel_table(width)), mix_input)
    coarse, twist, fine = call(
        table_kernel,
        (
            FAST((devices, devices), BF16),
            FAST((2, devices, positions), F32),
            FAST((2, positions, 2 * positions), BF16),
        ),
        [HBM] * 4,
        [NEAR] * 3,
        scratch=(pltpu.SemaphoreType.DMA((3,)),),
        limit=60 << 20,
        flops=1 << 30,
    )(
        items,
        table(coarse_table(devices)),
        twist.astype(np.float32),
        table(fine_tables(positions)),
    )
    items = exchange(items, devices)
    spectrum = call(
        position_kernel,
        FAST((rows, positions), BF16),
        [SCALAR] + [NEAR] * 4,
        NEAR,
        scratch=(pltpu.VMEM((rows, positions), F32), pltpu.VMEM((4, devices, 2 * positions), BF16)),
        limit=16 << 20,
    )(first, items, coarse, twist, fine)
    maps, weights = call(
        weight_kernel,
        (FAST(maps_shape, BF16), FAST(out_map.shape, BF16)),
        [HBM] * 4,
        [NEAR] * 2,
        scratch=(
            pltpu.VMEM((width, width), BF16),
            pltpu.VMEM(maps_shape, BF16),
            pltpu.SemaphoreType.DMA((3,)),
        ),
        limit=60 << 20,
        flops=1 << 30,
    )(spectrum, table(picker), group_maps, out_map)
    spectrum = exchange(spectrum, devices)
    pieces = 4
    return call(
        map_kernel,
        jax.ShapeDtypeStruct((sequences, positions, out_map.shape[1]), BF16),
        [NEAR] * 3,
        HBM,
        scratch=(
            pltpu.VMEM((sequences * positions, channels), BF16),
            pltpu.VMEM((pieces, sequences, positions, out_map.shape[1] // pieces), BF16),
            pltpu.SemaphoreType.DMA((pieces,)),
        ),
        limit=16 << 20,
    )(spectrum, maps, weights)


def solution(mesh):
    return jax.shard_map(
        per_device,
        mesh=mesh,
        in_specs=(P(None, AXES, None), P(), P()),
        out_specs=P(None, AXES, None),
        check_vma=False,
    )
```

time: 115 us -> 111 us (0.965)
  local copies, waits for them, and re-layouts: 3.94 us -> 0 us
  Pallas kernels: 6.49 us -> 10.1 us
  waiting for transfers between devices: 70.9 us -> 68 us
    unnamed x16 -> x0, local copies, waits for them, and re-layouts: 3.94 us -> none
    pallas_call x3 -> x5, Pallas kernels: 6.49 us -> 10.1 us  [the longest x1 2.6 us: per_device(): call(channel_kernel, FAST((rows, positions), BF16), [HBM, HBM], NEAR, scr...]
    all_to_all x2, waiting for transfers between devices: 70.9 us -> 68 us  [exchange(): lax.all_to_all(sent, AXES, split_axis=0, concat_axis=0, tiled=True)]
  transfers between devices with their start and end apart: 2 -> 2, of which waited for: 2 -> 2; matrix products, arithmetic and copies ran while one was open for 0% -> 0% of each run, Pallas kernels for 0% -> 3%
where the time goes in v2:
time: 111 us
  waiting for transfers between devices  68 us (61%)
  starting transfers between devices  32.7 us (29%)
  Pallas kernels  10.1 us (9%)
    all_to_all x2, waiting for transfers between devices, exchange(): lax.all_to_all(sent, AXES, split_axis=0, concat_axis=0, tiled=True)  68 us
    all_to_all x2, starting transfers between devices, exchange(): lax.all_to_all(sent, AXES, split_axis=0, concat_axis=0, tiled=True)  32.7 us
    pallas_call x1, Pallas kernels, per_device(): call(channel_kernel, FAST((rows, positions), BF16), [HBM, HBM], NEAR, scr...  2.6 us
    pallas_call x1, Pallas kernels, per_device(): call(map_kernel, jax.ShapeDtypeStruct((sequences, positions, out_map.shap...  2.3 us
  transfers between devices with their start and end apart: 2, of which 2 were waited for; matrix products, arithmetic and copies ran while one was open for 0% of the time, Pallas kernels for 3%

profile of v2, /device:TPU:1, one launch (start us, length us, event | category | flops | bytes accessed | tf_op | source)
XLA Modules:
  0.0 110.8 jit_solution(11008919918311346710)
XLA Ops:
  0.0 2.6 %shard_map.82.after_hbm = bf16[2048,128]{1,0:T(8,128)(2,1)} custom-call(bf16[128,128]{1,0:T(8,128)(2,1)} %constant.16.clone.table_hbm, bf16[4,128,512]{2,1,0:T(8,128)(2,1)} %signal_hbm.1), custom_call_target="tpu_custom_call" | custom-call | bytes 1048576 | tf_op jit(solution)/shard_map/pallas_call | solution.py:191
  2.6 24.3 %all-to-all-start = ((bf16[512,4,128]{2,1,0:T(4,128)(2,1)}), bf16[512,4,128]{2,1,0:T(4,128)(2,1)S(1)}, u32[]{:S(2)}, u32[]{:S(2)}) async-start(bf16[512,4,128]{2,1,0:T(4,128)(2,1)} %bitcast.1), calls=%async_computation | async-start | bytes 1048576 | tf_op jit(solution)/shard_map/all_to_all | solution.py:171
  26.9 1.2 %shard_map.83 = (bf16[512,512]{1,0:T(8,128)(2,1)S(1)}, f32[2,512,128]{2,1,0:T(8,128)S(1)}, bf16[2,128,256]{2,1,0:T(8,128)(2,1)S(1)}) custom-call(bf16[2048,128]{1,0:T(8,128)(2,1)} %shard_map.82.after_hbm, bf16[512,512]{1,0:T(8,128)(2,1)} %constant.17.clone.coarse_hbm, f32[2,512,128]{2,1,0:T(8,128)} %constant.18.clone.twist_hbm, ...), custom_call_target="tpu_custom_call" | custom-call | flops 1073741824 | bytes 1048576 | tf_op jit(solution)/shard_map/pallas_call | solution.py:203
  28.2 34.4 %all-to-all-done = bf16[512,4,128]{2,1,0:T(4,128)(2,1)S(1)} async-done(((bf16[512,4,128]{2,1,0:T(4,128)(2,1)}), bf16[512,4,128]{2,1,0:T(4,128)(2,1)S(1)}, u32[]{:S(2)}, u32[]{:S(2)}) %all-to-all-start) | async-done | bytes 524320 | tf_op jit(solution)/shard_map/all_to_all | solution.py:171
  62.6 2.1 %shard_map.84.after_hbm = bf16[2048,128]{1,0:T(8,128)(2,1)} custom-call(s32[1]{0:T(128)} %bitcast.edge_ref, bf16[2048,128]{1,0:T(8,128)(2,1)S(1)} %bitcast.5, bf16[512,512]{1,0:T(8,128)(2,1)S(1)} %get-tuple-element.10.coarse_ref, f32[2,512,128]{2,1,0:T(8,128)S(1)} %get-tuple-element.11.twist_ref, bf16[2,128,256]{2,1,0:T(8,128)(2,1)S(1)} %get-tuple-element.12.fine_ref), custom_call_target="tpu_custom_call" | custom-call | bytes 1048576 | tf_op jit(solution)/shard_map/pallas_call | solution.py:222
  64.6 8.4 %all-to-all-start.1 = ((bf16[512,4,128]{2,1,0:T(4,128)(2,1)}), bf16[512,4,128]{2,1,0:T(4,128)(2,1)S(1)}, u32[]{:S(2)}, u32[]{:S(2)}) async-start(bf16[512,4,128]{2,1,0:T(4,128)(2,1)} %bitcast.3), calls=%async_computation.1 | async-start | bytes 1048576 | tf_op jit(solution)/shard_map/all_to_all | solution.py:171
  73.0 1.9 %shard_map.85 = (bf16[4,128,128]{2,1,0:T(8,128)(2,1)S(1)}, bf16[512,2048]{1,0:T(8,128)(2,1)S(1)}) custom-call(bf16[2048,128]{1,0:T(8,128)(2,1)} %shard_map.84.after_hbm, bf16[128,128]{1,0:T(8,128)(2,1)} %constant.20.clone.picker_hbm, bf16[4,128,128]{2,1,0:T(8,128)(2,1)} %maps_hbm.1, bf16[512,2048]{1,0:T(8,128)(2,1)} %out_map_hbm.1), custom_call_target="tpu_custom_call" | custom-call | flops 1073741824 | bytes 1048576 | tf_op jit(solution)/shard_map/pallas_call | solution.py:230
  74.9 33.6 %all-to-all-done.1 = bf16[512,4,128]{2,1,0:T(4,128)(2,1)S(1)} async-done(((bf16[512,4,128]{2,1,0:T(4,128)(2,1)}), bf16[512,4,128]{2,1,0:T(4,128)(2,1)S(1)}, u32[]{:S(2)}, u32[]{:S(2)}) %all-to-all-start.1) | async-done | bytes 524320 | tf_op jit(solution)/shard_map/all_to_all | solution.py:171
  108.5 2.3 %shard_map.86 = bf16[4,128,2048]{2,1,0:T(8,128)(2,1)} custom-call(bf16[2048,128]{1,0:T(8,128)(2,1)S(1)} %bitcast.6, bf16[4,128,128]{2,1,0:T(8,128)(2,1)S(1)} %get-tuple-element.13.maps_ref, bf16[512,2048]{1,0:T(8,128)(2,1)S(1)} %get-tuple-element.14.out_map_ref), custom_call_target="tpu_custom_call" | custom-call | bytes 1048576 | tf_op jit(solution)/shard_map/pallas_call | solution.py:245
Async XLA Ops:
  2.6 60.0 %all-to-all-start = ((bf16[512,4,128]{2,1,0:T(4,128)(2,1)}), bf16[512,4,128]{2,1,0:T(4,128)(2,1)S(1)}, u32[]{:S(2)}, u32[]{:S(2)}) async-start(bf16[512,4,128]{2,1,0:T(4,128)(2,1)} %bitcast.1), calls=%async_computation | async-start | bytes 1048576 | tf_op jit(solution)/shard_map/all_to_all | solution.py:171
  64.6 43.9 %all-to-all-start.1 = ((bf16[512,4,128]{2,1,0:T(4,128)(2,1)}), bf16[512,4,128]{2,1,0:T(4,128)(2,1)S(1)}, u32[]{:S(2)}, u32[]{:S(2)}) async-start(bf16[512,4,128]{2,1,0:T(4,128)(2,1)} %bitcast.3), calls=%async_computation.1 | async-start | bytes 1048576 | tf_op jit(solution)/shard_map/all_to_all | solution.py:171

commit v3 on v2

--- a/solution.py
+++ b/solution.py
@@ -43,7 +43,7 @@
     return np.stack([np.block([[cosine, -sine]]), np.block([[-sine, -cosine]])])
 
 
-def channel_kernel(table_hbm, signal_hbm, out_ref, table_ref, signal_ref, sems):
+def channel_kernel(edge_ref, table_hbm, signal_hbm, out_ref, table_ref, signal_ref, sems):
     sequences, _, channels = signal_ref.shape
     width = table_ref.shape[0]
     groups = channels // width
@@ -61,24 +61,6 @@
             mapped = lax.dot_general(table_ref[...], block, NT, preferred_element_type=F32)
             start = (seq * groups + group) * width
             out_ref[start : start + width, :] = mapped.astype(BF16)
-
-
-def fetch(sources, targets, sems):
-    copies = [pltpu.make_async_copy(src, dst, sems.at[at]) for at, (src, dst) in enumerate(zip(sources, targets))]
-    for copy in copies:
-        copy.start()
-    for copy in copies:
-        copy.wait()
-
-
-def table_kernel(after_hbm, coarse_hbm, twist_hbm, fine_hbm, coarse_ref, twist_ref, fine_ref, sems):
-    fetch((coarse_hbm, twist_hbm, fine_hbm), (coarse_ref, twist_ref, fine_ref), sems)
-
-
-def weight_kernel(after_hbm, picker_hbm, maps_hbm, out_map_hbm, moved_ref, out_map_ref, picker_ref, maps_ref, sems):
-    fetch((picker_hbm, maps_hbm, out_map_hbm), (picker_ref, maps_ref, out_map_ref), sems)
-    for group in range(maps_ref.shape[0]):
-        moved_ref[group] = jnp.dot(picker_ref[...], maps_ref[group], preferred_element_type=F32).astype(BF16)
 
 
 def position_kernel(edge_ref, items_ref, coarse_ref, twist_ref, fine_ref, out_ref, wide_ref, spun_ref):
@@ -124,15 +106,16 @@
     out_ref[...] = wide_ref[...].astype(BF16)
 
 
-def map_kernel(spec_ref, maps_ref, out_map_ref, out_hbm, grouped_ref, mixed_ref, sems):
+def map_kernel(spec_ref, picker_ref, maps_ref, out_map_ref, out_hbm, grouped_ref, mixed_ref, sems):
     groups, width, _ = maps_ref.shape
     sequences, positions, _ = out_hbm.shape
-    for seq in range(sequences):
-        for group in range(groups):
+    for group in range(groups):
+        moved = jnp.dot(picker_ref[...], maps_ref[group], preferred_element_type=F32).astype(BF16)
+        for seq in range(sequences):
             start = (seq * groups + group) * width
             block = spec_ref[start : start + width, :]
             mapped = lax.dot_general(
-                block, maps_ref[group], (((0,), (0,)), ((), ())), preferred_element_type=F32
+                block, moved, (((0,), (0,)), ((), ())), preferred_element_type=F32
             )
             grouped_ref[seq * positions : (seq + 1) * positions, group * width : (group + 1) * width] = (
                 mapped.astype(BF16)
@@ -187,11 +170,10 @@
     picker = np.eye(width)[frequency_of_item(width)]
     first = (lax.axis_index("col") == 0).astype(jnp.int32).reshape(1)
 
-    maps_shape = group_maps.shape
     items = call(
         channel_kernel,
         FAST((rows, positions), BF16),
-        [HBM, HBM],
+        [SCALAR, HBM, HBM],
         NEAR,
         scratch=(
             pltpu.VMEM((width, width), BF16),
@@ -199,25 +181,7 @@
             pltpu.SemaphoreType.DMA((sequences + 1,)),
         ),
         limit=60 << 20,
-    )(table(channel_table(width)), mix_input)
-    coarse, twist, fine = call(
-        table_kernel,
-        (
-            FAST((devices, devices), BF16),
-            FAST((2, devices, positions), F32),
-            FAST((2, positions, 2 * positions), BF16),
-        ),
-        [HBM] * 4,
-        [NEAR] * 3,
-        scratch=(pltpu.SemaphoreType.DMA((3,)),),
-        limit=60 << 20,
-        flops=1 << 30,
-    )(
-        items,
-        table(coarse_table(devices)),
-        twist.astype(np.float32),
-        table(fine_tables(positions)),
-    )
+    )(first, table(channel_table(width)), mix_input)
     items = exchange(items, devices)
     spectrum = call(
         position_kernel,
@@ -226,26 +190,19 @@
         NEAR,
         scratch=(pltpu.VMEM((rows, positions), F32), pltpu.VMEM((4, devices, 2 * positions), BF16)),
         limit=16 << 20,
-    )(first, items, coarse, twist, fine)
-    maps, weights = call(
-        weight_kernel,
-        (FAST(maps_shape, BF16), FAST(out_map.shape, BF16)),
-        [HBM] * 4,
-        [NEAR] * 2,
-        scratch=(
-            pltpu.VMEM((width, width), BF16),
-            pltpu.VMEM(maps_shape, BF16),
-            pltpu.SemaphoreType.DMA((3,)),
-        ),
-        limit=60 << 20,
-        flops=1 << 30,
-    )(spectrum, table(picker), group_maps, out_map)
+    )(
+        first,
+        items,
+        table(coarse_table(devices)),
+        twist.astype(np.float32),
+        table(fine_tables(positions)),
+    )
     spectrum = exchange(spectrum, devices)
     pieces = 4
     return call(
         map_kernel,
         jax.ShapeDtypeStruct((sequences, positions, out_map.shape[1]), BF16),
-        [NEAR] * 3,
+        [NEAR] * 4,
         HBM,
         scratch=(
             pltpu.VMEM((sequences * positions, channels), BF16),
@@ -253,7 +210,7 @@
             pltpu.SemaphoreType.DMA((pieces,)),
         ),
         limit=16 << 20,
-    )(spectrum, maps, weights)
+    )(spectrum, table(picker), group_maps, out_map)
 
 
 def solution(mesh):

time: 111 us -> 110 us (level)
  blocking collectives: 0 us -> 104 us
  waiting for transfers between devices: 68 us -> 0 us
  starting transfers between devices: 32.7 us -> 0 us
  Pallas kernels: 10.1 us -> 6.02 us
    all_to_all x0 -> x2, blocking collectives: none -> 104 us  [exchange(): lax.all_to_all(sent, AXES, split_axis=0, concat_axis=0, tiled=True)]
    all_to_all x2 -> x0, waiting for transfers between devices: 68 us -> none  [exchange(): lax.all_to_all(sent, AXES, split_axis=0, concat_axis=0, tiled=True)]
    all_to_all x2 -> x0, starting transfers between devices: 32.7 us -> none  [exchange(): lax.all_to_all(sent, AXES, split_axis=0, concat_axis=0, tiled=True)]
    pallas_call x3 -> x1, Pallas kernels: 5.75 us -> 1.91 us  [per_device(): call(channel_kernel, FAST((rows, positions), BF16), [SCALAR, HBM, HBM], N...]
  transfers between devices with their start and end apart: 2 -> 0, of which waited for: 2 -> 0; matrix products, arithmetic and copies ran while one was open for 0% -> 0% of each run, Pallas kernels for 3% -> 0%
where the time goes in v3:
time: 110 us
  blocking collectives  104 us (95%)
  Pallas kernels  6.02 us (5%)
    all_to_all x2, blocking collectives, exchange(): lax.all_to_all(sent, AXES, split_axis=0, concat_axis=0, tiled=True)  104 us
    pallas_call x1, Pallas kernels, per_device(): call(map_kernel, jax.ShapeDtypeStruct((sequences, positions, out_map.shap...  2.83 us

profile of v3, /device:TPU:1, one launch (start us, length us, event | category | flops | bytes accessed | tf_op | source)
XLA Modules:
  0.0 110.2 jit_solution(8863687820747978584)
XLA Ops:
  0.0 0.0 copy-start.4
  0.0 0.0 copy-start.1
  0.0 0.0 copy-start.2
  0.0 1.9 %shard_map.82 = bf16[2048,128]{1,0:T(8,128)(2,1)S(1)} custom-call(s32[1]{0:T(128)} %bitcast.edge_ref, bf16[128,128]{1,0:T(8,128)(2,1)} %constant.16.clone.table_hbm, bf16[4,128,512]{2,1,0:T(8,128)(2,1)} %signal_hbm.1), custom_call_target="tpu_custom_call" | custom-call | bytes 1048576 | tf_op jit(solution)/shard_map/pallas_call | solution.py:173
  1.9 0.0 copy-start
  1.9 0.0 copy-start.3
  2.0 0.0 copy-start.5
  2.0 59.8 %all_to_all.10 = bf16[512,4,128]{2,1,0:T(4,128)(2,1)S(1)} all-to-all(bf16[512,4,128]{2,1,0:T(4,128)(2,1)S(1)} %bitcast.8), channel_id=1, replica_groups=mesh['row'=16,'col'=32] {'row','col'}, dimensions={0} | all-to-all | bytes 1048576 | tf_op jit(solution)/shard_map/all_to_all | solution.py:154
  61.7 0.0 copy-done.4
  61.7 0.0 copy-done.1
  61.7 0.0 copy-done.2
  61.7 1.3 %shard_map.83 = bf16[2048,128]{1,0:T(8,128)(2,1)S(1)} custom-call(s32[1]{0:T(128)} %bitcast.edge_ref, bf16[2048,128]{1,0:T(8,128)(2,1)S(1)} %bitcast.5, bf16[512,512]{1,0:T(8,128)(2,1)S(1)} %copy-done.2, f32[2,512,128]{2,1,0:T(8,128)S(1)} %copy-done.1, bf16[2,128,256]{2,1,0:T(8,128)(2,1)S(1)} %copy-done.4), custom_call_target="tpu_custom_call" | custom-call | bytes 1048576 | tf_op jit(solution)/shard_map/pallas_call | solution.py:186
  63.0 44.3 %all_to_all.11 = bf16[512,4,128]{2,1,0:T(4,128)(2,1)S(1)} all-to-all(bf16[512,4,128]{2,1,0:T(4,128)(2,1)S(1)} %bitcast.6), channel_id=1, replica_groups=mesh['row'=16,'col'=32] {'row','col'}, dimensions={0} | all-to-all | bytes 1048576 | tf_op jit(solution)/shard_map/all_to_all | solution.py:154
  107.4 0.0 copy-done
  107.4 0.0 copy-done.3
  107.4 0.0 copy-done.5
  107.4 2.8 %shard_map.84 = bf16[4,128,2048]{2,1,0:T(8,128)(2,1)} custom-call(bf16[2048,128]{1,0:T(8,128)(2,1)S(1)} %bitcast.7, bf16[128,128]{1,0:T(8,128)(2,1)S(1)} %copy-done.5, bf16[4,128,128]{2,1,0:T(8,128)(2,1)S(1)} %copy-done.3, bf16[512,2048]{1,0:T(8,128)(2,1)S(1)} %copy-done), custom_call_target="tpu_custom_call" | custom-call | bytes 1048576 | tf_op jit(solution)/shard_map/pallas_call | solution.py:202
Async XLA Ops:
  0.0 61.7 %copy-start.4 = (bf16[2,128,256]{2,1,0:T(8,128)(2,1)S(1)}, bf16[2,128,256]{2,1,0:T(8,128)(2,1)}, u32[]{:S(2)}) copy-start(bf16[2,128,256]{2,1,0:T(8,128)(2,1)} %constant.19.clone.fine_ref) | copy-start | bytes 393220
  0.0 61.7 %copy-start.1 = (f32[2,512,128]{2,1,0:T(8,128)S(1)}, f32[2,512,128]{2,1,0:T(8,128)}, u32[]{:S(2)}) copy-start(f32[2,512,128]{2,1,0:T(8,128)} %constant.18.clone.twist_ref) | copy-start | bytes 1572868
  0.0 61.7 %copy-start.2 = (bf16[512,512]{1,0:T(8,128)(2,1)S(1)}, bf16[512,512]{1,0:T(8,128)(2,1)}, u32[]{:S(2)}) copy-start(bf16[512,512]{1,0:T(8,128)(2,1)} %constant.17.clone.coarse_ref) | copy-start | bytes 1572868
  1.9 105.4 %copy-start = (bf16[512,2048]{1,0:T(8,128)(2,1)S(1)}, bf16[512,2048]{1,0:T(8,128)(2,1)}, u32[]{:S(2)}) copy-start(bf16[512,2048]{1,0:T(8,128)(2,1)} %out_map_ref.1) | copy-start | bytes 6291460
  1.9 105.4 %copy-start.3 = (bf16[4,128,128]{2,1,0:T(8,128)(2,1)S(1)}, bf16[4,128,128]{2,1,0:T(8,128)(2,1)}, u32[]{:S(2)}) copy-start(bf16[4,128,128]{2,1,0:T(8,128)(2,1)} %maps_ref.1) | copy-start | bytes 393220
  2.0 105.4 %copy-start.5 = (bf16[128,128]{1,0:T(8,128)(2,1)S(1)}, bf16[128,128]{1,0:T(8,128)(2,1)}, u32[]{:S(2)}) copy-start(bf16[128,128]{1,0:T(8,128)(2,1)} %constant.20.clone.picker_ref) | copy-start | bytes 98308

commit v4 on v3

--- a/solution.py
+++ b/solution.py
@@ -12,6 +12,7 @@
 AXES = ("row", "col")
 FAST = pltpu.VMEM
 F32, BF16 = jnp.float32, jnp.bfloat16
+CUTS = (0, 4, 8, 12, 14, 16)
 NT = (((1,), (1,)), ((), ()))
 
 
@@ -43,32 +44,12 @@
     return np.stack([np.block([[cosine, -sine]]), np.block([[-sine, -cosine]])])
 
 
-def channel_kernel(edge_ref, table_hbm, signal_hbm, out_ref, table_ref, signal_ref, sems):
-    sequences, _, channels = signal_ref.shape
-    width = table_ref.shape[0]
-    groups = channels // width
-    table_copy = pltpu.make_async_copy(table_hbm, table_ref, sems.at[sequences])
-    table_copy.start()
-    copies = []
-    for seq in range(sequences):
-        copies.append(pltpu.make_async_copy(signal_hbm.at[seq], signal_ref.at[seq], sems.at[seq]))
-        copies[seq].start()
-    table_copy.wait()
-    for seq in range(sequences):
-        copies[seq].wait()
-        for group in range(groups):
-            block = signal_ref[seq, :, group * width : (group + 1) * width]
-            mapped = lax.dot_general(table_ref[...], block, NT, preferred_element_type=F32)
-            start = (seq * groups + group) * width
-            out_ref[start : start + width, :] = mapped.astype(BF16)
-
-
-def position_kernel(edge_ref, items_ref, coarse_ref, twist_ref, fine_ref, out_ref, wide_ref, spun_ref):
+def position_kernel(items_ref, coarse_ref, twist_ref, fine_ref, out_ref, wide_ref, spun_ref):
     rows, lanes = items_ref.shape
     blocks = rows // 4
     half = blocks // 2
     quarters = blocks // lanes
-    edge = edge_ref[0]
+    edge = (lax.axis_index("col") == 0).astype(jnp.int32)
     wide_ref[...] = items_ref[...].astype(F32)
     for slot in range(2):
 
@@ -109,32 +90,27 @@
 def map_kernel(spec_ref, picker_ref, maps_ref, out_map_ref, out_hbm, grouped_ref, mixed_ref, sems):
     groups, width, _ = maps_ref.shape
     sequences, positions, _ = out_hbm.shape
+    maps = jnp.concatenate([maps_ref[group] for group in range(groups)], axis=1)
+    maps = jnp.dot(picker_ref[...], maps, preferred_element_type=F32).astype(BF16)
     for group in range(groups):
-        moved = jnp.dot(picker_ref[...], maps_ref[group], preferred_element_type=F32).astype(BF16)
-        for seq in range(sequences):
-            start = (seq * groups + group) * width
-            block = spec_ref[start : start + width, :]
-            mapped = lax.dot_general(
-                block, moved, (((0,), (0,)), ((), ())), preferred_element_type=F32
-            )
-            grouped_ref[seq * positions : (seq + 1) * positions, group * width : (group + 1) * width] = (
-                mapped.astype(BF16)
-            )
-    pieces, _, _, span = mixed_ref.shape
+        starts = [(seq * groups + group) * width for seq in range(sequences)]
+        block = jnp.concatenate([spec_ref[start : start + width, :] for start in starts], axis=1)
+        columns = slice(group * width, (group + 1) * width)
+        mapped = lax.dot_general(block, maps[:, columns], (((0,), (0,)), ((), ())), preferred_element_type=F32)
+        grouped_ref[:, columns] = mapped.astype(BF16)
     copies = []
-    for piece in range(pieces):
-        columns = slice(piece * span, (piece + 1) * span)
+    for at, (start, stop) in enumerate(zip(CUTS, CUTS[1:])):
+        columns = slice(start * width, stop * width)
         mixed = jnp.dot(grouped_ref[...], out_map_ref[:, columns], preferred_element_type=F32)
-        mixed_ref[piece] = mixed.astype(BF16).reshape(sequences, positions, span)
-        copies.append(pltpu.make_async_copy(mixed_ref.at[piece], out_hbm.at[:, :, columns], sems.at[piece]))
-        copies[piece].start()
+        mixed_ref[:, :, columns] = mixed.astype(BF16).reshape(sequences, positions, (stop - start) * width)
+        copies.append(pltpu.make_async_copy(mixed_ref.at[:, :, columns], out_hbm.at[:, :, columns], sems.at[at]))
+        copies[at].start()
     for copy in copies:
         copy.wait()
 
 
 HBM = pl.BlockSpec(memory_space=pl.ANY)
 NEAR = pl.BlockSpec(memory_space=pltpu.VMEM)
-SCALAR = pl.BlockSpec(memory_space=pltpu.SMEM)
 
 
 def call(kernel, out_shape, in_specs, out_specs, scratch=(), limit=None, flops=0):
@@ -160,6 +136,7 @@
     devices = lax.axis_size("row") * lax.axis_size("col")
     length = devices * positions
     rows = sequences * channels
+    assert out_map.shape[1] == CUTS[-1] * width
     assert rows == 4 * devices and positions == width and devices == 4 * positions
 
     def table(values):
@@ -168,37 +145,27 @@
     norm = 1.0 / math.sqrt(length * width)
     twist = norm * np.stack(turns(np.arange(devices), np.arange(positions), length))
     picker = np.eye(width)[frequency_of_item(width)]
-    first = (lax.axis_index("col") == 0).astype(jnp.int32).reshape(1)
 
-    items = call(
-        channel_kernel,
-        FAST((rows, positions), BF16),
-        [SCALAR, HBM, HBM],
-        NEAR,
-        scratch=(
-            pltpu.VMEM((width, width), BF16),
-            pltpu.VMEM(mix_input.shape, BF16),
-            pltpu.SemaphoreType.DMA((sequences + 1,)),
-        ),
-        limit=60 << 20,
-    )(first, table(channel_table(width)), mix_input)
+    signal = mix_input.reshape(sequences, positions, groups, width)
+    items = jnp.einsum(
+        "tj,sqgj->sgtq", table(channel_table(width)), signal, preferred_element_type=F32
+    ).astype(BF16)
+    items = items.reshape(rows, positions)
     items = exchange(items, devices)
     spectrum = call(
         position_kernel,
         FAST((rows, positions), BF16),
-        [SCALAR] + [NEAR] * 4,
+        [NEAR] * 4,
         NEAR,
         scratch=(pltpu.VMEM((rows, positions), F32), pltpu.VMEM((4, devices, 2 * positions), BF16)),
         limit=16 << 20,
     )(
-        first,
         items,
         table(coarse_table(devices)),
         twist.astype(np.float32),
         table(fine_tables(positions)),
     )
     spectrum = exchange(spectrum, devices)
-    pieces = 4
     return call(
         map_kernel,
         jax.ShapeDtypeStruct((sequences, positions, out_map.shape[1]), BF16),
@@ -206,8 +173,8 @@
         HBM,
         scratch=(
             pltpu.VMEM((sequences * positions, channels), BF16),
-            pltpu.VMEM((pieces, sequences, positions, out_map.shape[1] // pieces), BF16),
-            pltpu.SemaphoreType.DMA((pieces,)),
+            pltpu.VMEM((sequences, positions, out_map.shape[1]), BF16),
+            pltpu.SemaphoreType.DMA((len(CUTS) - 1,)),
         ),
         limit=16 << 20,
     )(spectrum, table(picker), group_maps, out_map)

time: 110 us -> 110 us (level)
  Pallas kernels: 6.02 us -> 3.66 us
    pallas_call x2 -> x1, Pallas kernels: 3.19 us -> 1.29 us  [per_device(): call(position_kernel, FAST((rows, positions), BF16), [NEAR] * 4, NEAR, sc...]
where the time goes in v4:
time: 110 us
  blocking collectives  104 us (95%)
  Pallas kernels  3.66 us (3%)
    all_to_all x2, blocking collectives, exchange(): lax.all_to_all(sent, AXES, split_axis=0, concat_axis=0, tiled=True)  104 us
    pallas_call x1, Pallas kernels, per_device(): call(map_kernel, jax.ShapeDtypeStruct((sequences, positions, out_map.shap...  2.37 us

profile of v4, /device:TPU:1, one launch (start us, length us, event | category | flops | bytes accessed | tf_op | source)
XLA Modules:
  0.0 109.9 jit_solution(12583604248927681076)
XLA Ops:
  0.0 0.0 copy-start
  0.0 0.0 copy-start.5
  0.0 0.0 copy-start.2
  0.0 0.0 copy-start.3
  0.0 1.0 copy-done
  1.0 1.0 convolution_convert_fusion
  2.1 0.0 copy-start.1
  2.1 0.0 copy-start.4
  2.1 0.0 copy-start.6
  2.1 59.8 %all_to_all.10 = bf16[512,4,128]{2,1,0:T(4,128)(2,1)S(1)} all-to-all(bf16[512,4,128]{2,1,0:T(4,128)(2,1)S(1)} %bitcast.20), channel_id=1, replica_groups=mesh['row'=16,'col'=32] {'row','col'}, dimensions={0} | all-to-all | bytes 1048576 | tf_op jit(solution)/shard_map/all_to_all | solution.py:130
  61.9 0.0 copy-done.5
  61.9 0.0 copy-done.2
  61.9 0.0 copy-done.3
  61.9 1.3 %shard_map.82 = bf16[2048,128]{1,0:T(8,128)(2,1)S(1)} custom-call(bf16[2048,128]{1,0:T(8,128)(2,1)S(1)} %bitcast.17, bf16[512,512]{1,0:T(8,128)(2,1)S(1)} %copy-done.3, f32[2,512,128]{2,1,0:T(8,128)S(1)} %copy-done.2, bf16[2,128,256]{2,1,0:T(8,128)(2,1)S(1)} %copy-done.5), custom_call_target="tpu_custom_call" | custom-call | bytes 1048576 | tf_op jit(solution)/shard_map/pallas_call | solution.py:155
  63.2 44.3 %all_to_all.11 = bf16[512,4,128]{2,1,0:T(4,128)(2,1)S(1)} all-to-all(bf16[512,4,128]{2,1,0:T(4,128)(2,1)S(1)} %bitcast.18), channel_id=1, replica_groups=mesh['row'=16,'col'=32] {'row','col'}, dimensions={0} | all-to-all | bytes 1048576 | tf_op jit(solution)/shard_map/all_to_all | solution.py:130
  107.5 0.0 copy-done.1
  107.5 0.0 copy-done.4
  107.5 0.0 copy-done.6
  107.5 2.4 %shard_map.83 = bf16[4,128,2048]{2,1,0:T(8,128)(2,1)} custom-call(bf16[2048,128]{1,0:T(8,128)(2,1)S(1)} %bitcast.19, bf16[128,128]{1,0:T(8,128)(2,1)S(1)} %copy-done.6, bf16[4,128,128]{2,1,0:T(8,128)(2,1)S(1)} %copy-done.4, bf16[512,2048]{1,0:T(8,128)(2,1)S(1)} %copy-done.1), custom_call_target="tpu_custom_call" | custom-call | bytes 1048576 | tf_op jit(solution)/shard_map/pallas_call | solution.py:169
Async XLA Ops:
  0.0 1.0 copy-start
  0.0 61.9 %copy-start.5 = (bf16[2,128,256]{2,1,0:T(8,128)(2,1)S(1)}, bf16[2,128,256]{2,1,0:T(8,128)(2,1)}, u32[]{:S(2)}) copy-start(bf16[2,128,256]{2,1,0:T(8,128)(2,1)} %constant.13.clone.fine_ref) | copy-start | bytes 393220
  0.0 61.9 %copy-start.2 = (f32[2,512,128]{2,1,0:T(8,128)S(1)}, f32[2,512,128]{2,1,0:T(8,128)}, u32[]{:S(2)}) copy-start(f32[2,512,128]{2,1,0:T(8,128)} %constant.12.clone.twist_ref) | copy-start | bytes 1572868
  0.0 61.9 %copy-start.3 = (bf16[512,512]{1,0:T(8,128)(2,1)S(1)}, bf16[512,512]{1,0:T(8,128)(2,1)}, u32[]{:S(2)}) copy-start(bf16[512,512]{1,0:T(8,128)(2,1)} %constant.11.clone.coarse_ref) | copy-start | bytes 1572868
  2.1 105.4 %copy-start.1 = (bf16[512,2048]{1,0:T(8,128)(2,1)S(1)}, bf16[512,2048]{1,0:T(8,128)(2,1)}, u32[]{:S(2)}) copy-start(bf16[512,2048]{1,0:T(8,128)(2,1)} %out_map_ref.1) | copy-start | bytes 6291460
  2.1 105.4 %copy-start.4 = (bf16[4,128,128]{2,1,0:T(8,128)(2,1)S(1)}, bf16[4,128,128]{2,1,0:T(8,128)(2,1)}, u32[]{:S(2)}) copy-start(bf16[4,128,128]{2,1,0:T(8,128)(2,1)} %maps_ref.1) | copy-start | bytes 393220
  2.1 105.4 %copy-start.6 = (bf16[128,128]{1,0:T(8,128)(2,1)S(1)}, bf16[128,128]{1,0:T(8,128)(2,1)}, u32[]{:S(2)}) copy-start(bf16[128,128]{1,0:T(8,128)(2,1)} %constant.14.clone.picker_ref) | copy-start | bytes 98308

commit v5 on v4

--- a/solution.py
+++ b/solution.py
@@ -42,6 +42,24 @@
 def fine_tables(count):
     cosine, sine = turns(np.arange(count), np.arange(count), count)
     return np.stack([np.block([[cosine, -sine]]), np.block([[-sine, -cosine]])])
+
+
+def channel_kernel(table_hbm, signal_hbm, out_ref, table_ref, signal_ref, sems):
+    sequences, positions, channels = signal_ref.shape
+    span = table_ref.shape[0]
+    signal_copy = pltpu.make_async_copy(signal_hbm, signal_ref, sems.at[0])
+    table_copy = pltpu.make_async_copy(table_hbm, table_ref, sems.at[1])
+    signal_copy.start()
+    table_copy.start()
+    signal_copy.wait()
+    table_copy.wait()
+    for first in range(0, sequences, 2):
+        for start in range(0, channels, span):
+            block = jnp.concatenate([signal_ref[first + at, :, start : start + span] for at in range(2)], axis=0)
+            mapped = lax.dot_general(table_ref[...], block, NT, preferred_element_type=F32).astype(BF16)
+            for at in range(2):
+                top = (first + at) * channels + start
+                out_ref[top : top + span, :] = mapped[:, at * positions : (at + 1) * positions]
 
 
 def position_kernel(items_ref, coarse_ref, twist_ref, fine_ref, out_ref, wide_ref, spun_ref):
@@ -146,11 +164,18 @@
     twist = norm * np.stack(turns(np.arange(devices), np.arange(positions), length))
     picker = np.eye(width)[frequency_of_item(width)]
 
-    signal = mix_input.reshape(sequences, positions, groups, width)
-    items = jnp.einsum(
-        "tj,sqgj->sgtq", table(channel_table(width)), signal, preferred_element_type=F32
-    ).astype(BF16)
-    items = items.reshape(rows, positions)
+    items = call(
+        channel_kernel,
+        FAST((rows, positions), BF16),
+        [HBM, HBM],
+        NEAR,
+        scratch=(
+            pltpu.VMEM((2 * width, 2 * width), BF16),
+            pltpu.VMEM(mix_input.shape, BF16),
+            pltpu.SemaphoreType.DMA((2,)),
+        ),
+        limit=60 << 20,
+    )(table(np.kron(np.eye(2), channel_table(width))), mix_input)
     items = exchange(items, devices)
     spectrum = call(
         position_kernel,

time: 110 us -> 110 us (level)
  Pallas kernels: 3.66 us -> 5.17 us
    pallas_call x0 -> x1, Pallas kernels: none -> 1.51 us  [per_device(): call(channel_kernel, FAST((rows, positions), BF16), [HBM, HBM], NEAR, scr...]
where the time goes in v5:
time: 110 us; the launch traced here: 109 us
  blocking collectives  104 us (95%)
  Pallas kernels  5.17 us (5%)
    all_to_all x2, blocking collectives, exchange(): lax.all_to_all(sent, AXES, split_axis=0, concat_axis=0, tiled=True)  104 us
    pallas_call x1, Pallas kernels, per_device(): call(map_kernel, jax.ShapeDtypeStruct((sequences, positions, out_map.shap...  2.37 us

profile of v5, /device:TPU:1, one launch (start us, length us, event | category | flops | bytes accessed | tf_op | source)
XLA Modules:
  0.0 109.3 jit_solution(6644794474095912029)
XLA Ops:
  0.0 0.0 copy-start.4
  0.0 0.0 copy-start.1
  0.0 0.0 copy-start.2
  0.0 1.5 %shard_map.82 = bf16[2048,128]{1,0:T(8,128)(2,1)S(1)} custom-call(bf16[256,256]{1,0:T(8,128)(2,1)} %constant.10.clone.table_hbm, bf16[4,128,512]{2,1,0:T(8,128)(2,1)} %signal_hbm.1), custom_call_target="tpu_custom_call" | custom-call | bytes 1048576 | tf_op jit(solution)/shard_map/pallas_call | solution.py:167
  1.5 0.0 copy-start
  1.5 0.0 copy-start.3
  1.6 0.0 copy-start.5
  1.6 59.8 %all_to_all.10 = bf16[512,4,128]{2,1,0:T(4,128)(2,1)S(1)} all-to-all(bf16[512,4,128]{2,1,0:T(4,128)(2,1)S(1)} %bitcast.7), channel_id=1, replica_groups=mesh['row'=16,'col'=32] {'row','col'}, dimensions={0} | all-to-all | bytes 1048576 | tf_op jit(solution)/shard_map/all_to_all | solution.py:148
  61.3 0.0 copy-done.4
  61.3 0.0 copy-done.1
  61.3 0.0 copy-done.2
  61.3 1.3 %shard_map.83 = bf16[2048,128]{1,0:T(8,128)(2,1)S(1)} custom-call(bf16[2048,128]{1,0:T(8,128)(2,1)S(1)} %bitcast.4, bf16[512,512]{1,0:T(8,128)(2,1)S(1)} %copy-done.2, f32[2,512,128]{2,1,0:T(8,128)S(1)} %copy-done.1, bf16[2,128,256]{2,1,0:T(8,128)(2,1)S(1)} %copy-done.4), custom_call_target="tpu_custom_call" | custom-call | bytes 1048576 | tf_op jit(solution)/shard_map/pallas_call | solution.py:180
  62.6 44.3 %all_to_all.11 = bf16[512,4,128]{2,1,0:T(4,128)(2,1)S(1)} all-to-all(bf16[512,4,128]{2,1,0:T(4,128)(2,1)S(1)} %bitcast.5), channel_id=1, replica_groups=mesh['row'=16,'col'=32] {'row','col'}, dimensions={0} | all-to-all | bytes 1048576 | tf_op jit(solution)/shard_map/all_to_all | solution.py:148
  107.0 0.0 copy-done
  107.0 0.0 copy-done.3
  107.0 0.0 copy-done.5
  107.0 2.4 %shard_map.84 = bf16[4,128,2048]{2,1,0:T(8,128)(2,1)} custom-call(bf16[2048,128]{1,0:T(8,128)(2,1)S(1)} %bitcast.6, bf16[128,128]{1,0:T(8,128)(2,1)S(1)} %copy-done.5, bf16[4,128,128]{2,1,0:T(8,128)(2,1)S(1)} %copy-done.3, bf16[512,2048]{1,0:T(8,128)(2,1)S(1)} %copy-done), custom_call_target="tpu_custom_call" | custom-call | bytes 1048576 | tf_op jit(solution)/shard_map/pallas_call | solution.py:194
Async XLA Ops:
  0.0 61.3 %copy-start.4 = (bf16[2,128,256]{2,1,0:T(8,128)(2,1)S(1)}, bf16[2,128,256]{2,1,0:T(8,128)(2,1)}, u32[]{:S(2)}) copy-start(bf16[2,128,256]{2,1,0:T(8,128)(2,1)} %constant.13.clone.fine_ref) | copy-start | bytes 393220
  0.0 61.3 %copy-start.1 = (f32[2,512,128]{2,1,0:T(8,128)S(1)}, f32[2,512,128]{2,1,0:T(8,128)}, u32[]{:S(2)}) copy-start(f32[2,512,128]{2,1,0:T(8,128)} %constant.12.clone.twist_ref) | copy-start | bytes 1572868
  0.0 61.3 %copy-start.2 = (bf16[512,512]{1,0:T(8,128)(2,1)S(1)}, bf16[512,512]{1,0:T(8,128)(2,1)}, u32[]{:S(2)}) copy-start(bf16[512,512]{1,0:T(8,128)(2,1)} %constant.11.clone.coarse_ref) | copy-start | bytes 1572868
  1.5 105.4 %copy-start = (bf16[512,2048]{1,0:T(8,128)(2,1)S(1)}, bf16[512,2048]{1,0:T(8,128)(2,1)}, u32[]{:S(2)}) copy-start(bf16[512,2048]{1,0:T(8,128)(2,1)} %out_map_ref.1) | copy-start | bytes 6291460
  1.5 105.4 %copy-start.3 = (bf16[4,128,128]{2,1,0:T(8,128)(2,1)S(1)}, bf16[4,128,128]{2,1,0:T(8,128)(2,1)}, u32[]{:S(2)}) copy-start(bf16[4,128,128]{2,1,0:T(8,128)(2,1)} %maps_ref.1) | copy-start | bytes 393220
  1.6 105.4 %copy-start.5 = (bf16[128,128]{1,0:T(8,128)(2,1)S(1)}, bf16[128,128]{1,0:T(8,128)(2,1)}, u32[]{:S(2)}) copy-start(bf16[128,128]{1,0:T(8,128)(2,1)} %constant.14.clone.picker_ref) | copy-start | bytes 98308

commit v6 on v5

--- a/solution.py
+++ b/solution.py
@@ -62,7 +62,7 @@
                 out_ref[top : top + span, :] = mapped[:, at * positions : (at + 1) * positions]
 
 
-def position_kernel(items_ref, coarse_ref, twist_ref, fine_ref, out_ref, wide_ref, spun_ref):
+def position_kernel(items_ref, coarse_ref, twist_ref, fine_ref, out_hbm, wide_ref, spun_ref, out_ref, sems):
     rows, lanes = items_ref.shape
     blocks = rows // 4
     half = blocks // 2
@@ -102,14 +102,34 @@
                 wide_ref[pl.ds(4 * quarter + 2 * slot + part, lanes, stride=4 * quarters), :] = results[part][
                     :, quarter * lanes : (quarter + 1) * lanes
                 ]
-    out_ref[...] = wide_ref[...].astype(BF16)
-
-
-def map_kernel(spec_ref, picker_ref, maps_ref, out_map_ref, out_hbm, grouped_ref, mixed_ref, sems):
+    copies = []
+    for piece in range(4):
+        span = slice(piece * (rows // 4), (piece + 1) * (rows // 4))
+        out_ref[span, :] = wide_ref[span, :].astype(BF16)
+        copies.append(pltpu.make_async_copy(out_ref.at[span], out_hbm.at[span], sems.at[piece]))
+        copies[piece].start()
+    for copy in copies:
+        copy.wait()
+
+
+def weight_kernel(after_hbm, picker_hbm, maps_hbm, out_map_hbm, moved_ref, out_map_ref, picker_ref, maps_ref, sems):
+    pairs = ((picker_hbm, picker_ref), (maps_hbm, maps_ref), (out_map_hbm, out_map_ref))
+    copies = [pltpu.make_async_copy(source, target, sems.at[at]) for at, (source, target) in enumerate(pairs)]
+    for copy in copies:
+        copy.start()
+    for copy in copies:
+        copy.wait()
     groups, width, _ = maps_ref.shape
+    for group in range(groups):
+        mapped = jnp.dot(picker_ref[...], maps_ref[group], preferred_element_type=F32)
+        moved_ref[:, group * width : (group + 1) * width] = mapped.astype(BF16)
+
+
+def map_kernel(spec_ref, maps_ref, out_map_ref, out_hbm, grouped_ref, mixed_ref, sems):
     sequences, positions, _ = out_hbm.shape
-    maps = jnp.concatenate([maps_ref[group] for group in range(groups)], axis=1)
-    maps = jnp.dot(picker_ref[...], maps, preferred_element_type=F32).astype(BF16)
+    width, channels = maps_ref.shape
+    groups = channels // width
+    maps = maps_ref[...]
     for group in range(groups):
         starts = [(seq * groups + group) * width for seq in range(sequences)]
         block = jnp.concatenate([spec_ref[start : start + width, :] for start in starts], axis=1)
@@ -179,10 +199,15 @@
     items = exchange(items, devices)
     spectrum = call(
         position_kernel,
-        FAST((rows, positions), BF16),
+        jax.ShapeDtypeStruct((rows, positions), BF16),
         [NEAR] * 4,
-        NEAR,
-        scratch=(pltpu.VMEM((rows, positions), F32), pltpu.VMEM((4, devices, 2 * positions), BF16)),
+        HBM,
+        scratch=(
+            pltpu.VMEM((rows, positions), F32),
+            pltpu.VMEM((4, devices, 2 * positions), BF16),
+            pltpu.VMEM((rows, positions), BF16),
+            pltpu.SemaphoreType.DMA((4,)),
+        ),
         limit=16 << 20,
     )(
         items,
@@ -190,11 +215,24 @@
         twist.astype(np.float32),
         table(fine_tables(positions)),
     )
+    maps, weights = call(
+        weight_kernel,
+        (FAST((width, channels), BF16), FAST(out_map.shape, BF16)),
+        [HBM] * 4,
+        [NEAR] * 2,
+        scratch=(
+            pltpu.VMEM((width, width), BF16),
+            pltpu.VMEM(group_maps.shape, BF16),
+            pltpu.SemaphoreType.DMA((3,)),
+        ),
+        limit=60 << 20,
+        flops=1 << 30,
+    )(spectrum, table(picker), group_maps, out_map)
     spectrum = exchange(spectrum, devices)
     return call(
         map_kernel,
         jax.ShapeDtypeStruct((sequences, positions, out_map.shape[1]), BF16),
-        [NEAR] * 4,
+        [NEAR] * 3,
         HBM,
         scratch=(
             pltpu.VMEM((sequences * positions, channels), BF16),
@@ -202,7 +240,7 @@
             pltpu.SemaphoreType.DMA((len(CUTS) - 1,)),
         ),
         limit=16 << 20,
-    )(spectrum, table(picker), group_maps, out_map)
+    )(spectrum, maps, weights)
 
 
 def solution(mesh):

time: 110 us -> 110 us (level)
  blocking collectives: 104 us -> 59.8 us
  waiting for transfers between devices: 0 us -> 33.7 us
  starting transfers between devices: 0 us -> 8.39 us
  Pallas kernels: 5.17 us -> 7.69 us
    all_to_all x2 -> x1, blocking collectives: 104 us -> 59.8 us  [exchange(): lax.all_to_all(sent, AXES, split_axis=0, concat_axis=0, tiled=True)]
    all_to_all x0 -> x1, waiting for transfers between devices: none -> 33.7 us  [exchange(): lax.all_to_all(sent, AXES, split_axis=0, concat_axis=0, tiled=True)]
    all_to_all x0 -> x1, starting transfers between devices: none -> 8.39 us  [exchange(): lax.all_to_all(sent, AXES, split_axis=0, concat_axis=0, tiled=True)]
    pallas_call x1 -> x2, Pallas kernels: 1.29 us -> 3.92 us  [the longest x1 2.02 us: per_device(): call(position_kernel, jax.ShapeDtypeStruct((rows, positions), BF16), [NEA...]
  transfers between devices with their start and end apart: 0 -> 1, of which waited for: 0 -> 1; matrix products, arithmetic and copies ran while one was open for 0% -> 0% of each run, Pallas kernels for 0% -> 2%
where the time goes in v6:
time: 110 us
  blocking collectives  59.8 us (54%)
  waiting for transfers between devices  33.7 us (31%)
  starting transfers between devices  8.39 us (8%)
  Pallas kernels  7.69 us (7%)
    all_to_all x1, blocking collectives, exchange(): lax.all_to_all(sent, AXES, split_axis=0, concat_axis=0, tiled=True)  59.8 us
    all_to_all x1, waiting for transfers between devices, exchange(): lax.all_to_all(sent, AXES, split_axis=0, concat_axis=0, tiled=True)  33.7 us
    all_to_all x1, starting transfers between devices, exchange(): lax.all_to_all(sent, AXES, split_axis=0, concat_axis=0, tiled=True)  8.39 us
    pallas_call x1, Pallas kernels, per_device(): call(map_kernel, jax.ShapeDtypeStruct((sequences, positions, out_map.shap...  2.26 us
  transfers between devices with their start and end apart: 1, of which 1 were waited for; matrix products, arithmetic and copies ran while one was open for 0% of the time, Pallas kernels for 2%

profile of v6, /device:TPU:1, one launch (start us, length us, event | category | flops | bytes accessed | tf_op | source)
XLA Modules:
  0.0 109.6 jit_solution(3897867964732615467)
XLA Ops:
  0.0 0.0 copy-start.2
  0.0 0.0 copy-start
  0.0 0.0 copy-start.1
  0.0 1.5 %shard_map.82 = bf16[2048,128]{1,0:T(8,128)(2,1)S(1)} custom-call(bf16[256,256]{1,0:T(8,128)(2,1)} %constant.10.clone.table_hbm, bf16[4,128,512]{2,1,0:T(8,128)(2,1)} %signal_hbm.1), custom_call_target="tpu_custom_call" | custom-call | bytes 1048576 | tf_op jit(solution)/shard_map/pallas_call | solution.py:187
  1.5 59.8 %all_to_all.10 = bf16[512,4,128]{2,1,0:T(4,128)(2,1)S(1)} all-to-all(bf16[512,4,128]{2,1,0:T(4,128)(2,1)S(1)} %bitcast.6), channel_id=1, replica_groups=mesh['row'=16,'col'=32] {'row','col'}, dimensions={0} | all-to-all | bytes 1048576 | tf_op jit(solution)/shard_map/all_to_all | solution.py:168
  61.3 0.0 copy-done.2
  61.3 0.0 copy-done
  61.3 0.0 copy-done.1
  61.3 2.0 %shard_map.83.after_hbm = bf16[2048,128]{1,0:T(8,128)(2,1)} custom-call(bf16[2048,128]{1,0:T(8,128)(2,1)S(1)} %bitcast.5, bf16[512,512]{1,0:T(8,128)(2,1)S(1)} %copy-done.1, f32[2,512,128]{2,1,0:T(8,128)S(1)} %copy-done, bf16[2,128,256]{2,1,0:T(8,128)(2,1)S(1)} %copy-done.2), custom_call_target="tpu_custom_call" | custom-call | bytes 1048576 | tf_op jit(solution)/shard_map/pallas_call | solution.py:200
  63.3 8.4 %all-to-all-start.1 = ((bf16[512,4,128]{2,1,0:T(4,128)(2,1)}), bf16[512,4,128]{2,1,0:T(4,128)(2,1)S(1)}, u32[]{:S(2)}, u32[]{:S(2)}) async-start(bf16[512,4,128]{2,1,0:T(4,128)(2,1)} %bitcast.2), calls=%async_computation.1 | async-start | bytes 1048576 | tf_op jit(solution)/shard_map/all_to_all | solution.py:168
  71.7 1.9 %shard_map.84 = (bf16[128,512]{1,0:T(8,128)(2,1)S(1)}, bf16[512,2048]{1,0:T(8,128)(2,1)S(1)}) custom-call(bf16[2048,128]{1,0:T(8,128)(2,1)} %shard_map.83.after_hbm, bf16[128,128]{1,0:T(8,128)(2,1)} %constant.14.clone.picker_hbm, bf16[4,128,128]{2,1,0:T(8,128)(2,1)} %maps_hbm.1, bf16[512,2048]{1,0:T(8,128)(2,1)} %out_map_hbm.1), custom_call_target="tpu_custom_call" | custom-call | flops 1073741824 | bytes 1048576 | tf_op jit(solution)/shard_map/pallas_call | solution.py:218
  73.6 33.7 %all-to-all-done.1 = bf16[512,4,128]{2,1,0:T(4,128)(2,1)S(1)} async-done(((bf16[512,4,128]{2,1,0:T(4,128)(2,1)}), bf16[512,4,128]{2,1,0:T(4,128)(2,1)S(1)}, u32[]{:S(2)}, u32[]{:S(2)}) %all-to-all-start.1) | async-done | bytes 524320 | tf_op jit(solution)/shard_map/all_to_all | solution.py:168
  107.4 2.3 %shard_map.85 = bf16[4,128,2048]{2,1,0:T(8,128)(2,1)} custom-call(bf16[2048,128]{1,0:T(8,128)(2,1)S(1)} %bitcast.4, bf16[128,512]{1,0:T(8,128)(2,1)S(1)} %get-tuple-element.7.maps_ref, bf16[512,2048]{1,0:T(8,128)(2,1)S(1)} %get-tuple-element.8.out_map_ref), custom_call_target="tpu_custom_call" | custom-call | bytes 1048576 | tf_op jit(solution)/shard_map/pallas_call | solution.py:232
Async XLA Ops:
  0.0 61.3 %copy-start.2 = (bf16[2,128,256]{2,1,0:T(8,128)(2,1)S(1)}, bf16[2,128,256]{2,1,0:T(8,128)(2,1)}, u32[]{:S(2)}) copy-start(bf16[2,128,256]{2,1,0:T(8,128)(2,1)} %constant.13.clone.fine_ref) | copy-start | bytes 393220
  0.0 61.3 %copy-start = (f32[2,512,128]{2,1,0:T(8,128)S(1)}, f32[2,512,128]{2,1,0:T(8,128)}, u32[]{:S(2)}) copy-start(f32[2,512,128]{2,1,0:T(8,128)} %constant.12.clone.twist_ref) | copy-start | bytes 1572868
  0.0 61.3 %copy-start.1 = (bf16[512,512]{1,0:T(8,128)(2,1)S(1)}, bf16[512,512]{1,0:T(8,128)(2,1)}, u32[]{:S(2)}) copy-start(bf16[512,512]{1,0:T(8,128)(2,1)} %constant.11.clone.coarse_ref) | copy-start | bytes 1572868
  63.3 44.0 %all-to-all-start.1 = ((bf16[512,4,128]{2,1,0:T(4,128)(2,1)}), bf16[512,4,128]{2,1,0:T(4,128)(2,1)S(1)}, u32[]{:S(2)}, u32[]{:S(2)}) async-start(bf16[512,4,128]{2,1,0:T(4,128)(2,1)} %bitcast.2), calls=%async_computation.1 | async-start | bytes 1048576 | tf_op jit(solution)/shard_map/all_to_all | solution.py:168
